TPU v7x, 512 devices: a whole 4x4x16 slice. The times are simulated.
512 devices in a mesh: kv: 64 (over z, y), tp: 8 (over x, core).
Axes of the slice: x: 4, y: 4, z: 16, core: 2. Of those that a mesh axis runs over, the one named last changes fastest.
Arguments:
- residual_in: bfloat16 [384, 2048], P('kv', 'tp'), may hold values from -36 to 36
- gain_pre: float32 [2048], P('tp'), may hold values from 0.1 to 1.9
- gate_pre: bfloat16 [2048, 5632], P('tp', 'kv'), may hold values from -0.125 to 0.125
- up_pre: bfloat16 [2048, 5632], P('tp', 'kv'), may hold values from -0.125 to 0.125
- down_pre: bfloat16 [5632, 2048], P('kv', 'tp'), may hold values from -0.078125 to 0.078125
- gain_mix: float32 [2048], replicated, may hold values from 0.1 to 1.9
- query_weight: bfloat16 [2048, 2048], P('kv', 'tp'), may hold values from -0.125 to 0.125
- forget_weight: bfloat16 [2048, 2048], P('kv', 'tp'), may hold values from -0.125 to 0.125
- value_weight: bfloat16 [2048, 2048], P('kv', 'tp'), may hold values from -0.125 to 0.125
- outgate_weight: bfloat16 [2048, 2048], P('kv', 'tp'), may hold values from -0.125 to 0.125
- lower_bound: float32 [2048], P('tp'), may hold values from 0.05 to 0.95
- head_gain: float32 [2048], P('tp'), may hold values from 0.1 to 1.9
- out_weight: bfloat16 [2048, 2048], P('tp'), may hold values from -0.125 to 0.125
- gain_post: float32 [2048], P('tp'), may hold values from 0.1 to 1.9
- gate_post: bfloat16 [2048, 5632], P('tp', 'kv'), may hold values from -0.125 to 0.125
- up_post: bfloat16 [2048, 5632], P('tp', 'kv'), may hold values from -0.125 to 0.125
- down_post: bfloat16 [5632, 2048], P('kv', 'tp'), may hold values from -0.078125 to 0.078125
- memory_state: float32 [384, 16, 128, 128], P('kv', 'tp'), may hold values from -4 to 4
Outputs:
- layer_out: bfloat16 [384, 2048], P('kv', 'tp')
- next_state: float32 [384, 16, 128, 128], P('kv', 'tp')
All inputs are finite; a program needn't handle non-finite values.
Results may differ from a plain program's by a relative error of at most 0.014.
Values may be sent and summed in bfloat16 or wider, within the bound.
No kernel may reach another device: no remote copies, remote signals or barrier semaphores. Data moves between devices by JAX's collectives and lax.ppermute only.
A program may use at most 64 MiB of HBM per device.

v0:
```python
import jax
import jax.numpy as jnp
from jax import lax
from jax.sharding import PartitionSpec as P

D = 2048
HEAD_DIM = 128


EPSILON = 1e-06


def joined_along(tiles, dim):
    tiles = jnp.moveaxis(tiles, 0, dim)
    shape = tiles.shape
    return tiles.reshape(*shape[:dim], shape[dim] * shape[dim + 1], *shape[dim + 2 :])


def sent_to_all(array, axis):
    copies = jnp.broadcast_to(array, (lax.axis_size(axis), *array.shape))
    return lax.all_to_all(copies, axis, split_axis=0, concat_axis=0, tiled=True)


def collect(array, axis, dim):
    return joined_along(sent_to_all(array, axis), dim)


def cut_along(array, dim, size):
    shape = array.shape
    tiles = array.reshape(*shape[:dim], size, shape[dim] // size, *shape[dim + 1 :])
    return jnp.moveaxis(tiles, dim, 0)


def sent_and_summed(array, axis, dim):
    tiles = cut_along(array, dim, lax.axis_size(axis))
    arrived = lax.all_to_all(tiles, axis, split_axis=0, concat_axis=0, tiled=True)
    return arrived.astype(jnp.float32).sum(axis=0)


def sent_together(arrays, axis, dim, along):
    columns = [a.reshape(*a.shape[:along], -1) for a in arrays]
    both = jnp.concatenate(columns, axis=along)
    filled, at, done = (sent_and_summed(both, axis, dim), 0, [])
    for a, column in zip(arrays, columns):
        section = filled[..., at : at + column.shape[along]]
        done.append(section.reshape(*section.shape[:along], *a.shape[along:]))
        at += column.shape[along]
    return tuple(done)


def in_one_piece(arrays, axis, dim, along):
    widths = [a.shape[along] for a in arrays]
    both = jnp.concatenate(arrays, axis=along)
    filled = lax.all_gather(both, axis, axis=dim, tiled=True)
    return tuple(jnp.split(filled, [sum(widths[:k]) for k in range(1, len(widths))], axis=along))


def channel_mixer(row_block, gain_vec, gate_weight, up_weight, down_weight):
    gathered = collect(row_block, "kv", 0)
    widened = gathered.astype(jnp.float32)
    part_squares = jnp.sum(widened * widened, axis=1)
    scaled = (widened * gain_vec).astype(jnp.bfloat16)
    gate_part = jnp.dot(scaled, gate_weight, preferred_element_type=jnp.float32)
    up_part = jnp.dot(scaled, up_weight, preferred_element_type=jnp.float32)
    gate_share, up_share, square_share = sent_together(
        (
            gate_part.astype(jnp.bfloat16),
            up_part.astype(jnp.bfloat16),
            part_squares.astype(jnp.bfloat16),
        ),
        "tp",
        0,
        1,
    )
    share_inverse = lax.rsqrt(square_share / D + EPSILON)[:, None]
    hidden_share = (jax.nn.silu(gate_share * share_inverse) * (up_share * share_inverse)).astype(
        jnp.bfloat16
    )
    hidden = collect(hidden_share, "tp", 0)
    return sent_and_summed(
        jnp.dot(hidden, down_weight, preferred_element_type=jnp.float32).astype(jnp.bfloat16),
        "kv",
        0,
    )


def token_mixer(
    stream_a,
    gain_mix,
    query_weight,
    forget_weight,
    value_weight,
    outgate_weight,
    lower_bound,
    head_gain,
    out_weight,
    memory_state,
):
    full_rows = collect(stream_a, "tp", 1)
    widened = full_rows.astype(jnp.float32)
    inverse = lax.rsqrt(jnp.mean(widened * widened, axis=1, keepdims=True) + EPSILON)
    scaled = (widened * gain_mix).astype(jnp.bfloat16)
    weights = (query_weight, forget_weight, value_weight, outgate_weight)
    full_weights = in_one_piece((weights[0], weights[1], weights[2], weights[3]), "kv", 0, 1)
    projected = jnp.concatenate(
        [
            jnp.dot(scaled, weight_rows, preferred_element_type=jnp.float32)
            for weight_rows in full_weights
        ],
        axis=1,
    )
    projected = projected * inverse
    seq_rows = scaled.shape[0]
    local_heads = query_weight.shape[1] // HEAD_DIM
    reshaped = projected.reshape(seq_rows, 4, local_heads, HEAD_DIM)
    query_pre = reshaped[:, 0]
    forget_pre = reshaped[:, 1]
    value_pre = reshaped[:, 2]
    outgate_pre = reshaped[:, 3]
    floor_rate = lower_bound.reshape(local_heads, HEAD_DIM)
    log_keep = jnp.logaddexp(
        jnp.log(floor_rate), jnp.log1p(-floor_rate) + jax.nn.log_sigmoid(forget_pre)
    )
    inject = (1.0 - floor_rate) * jax.nn.sigmoid(-forget_pre)
    next_state = (
        jnp.exp(log_keep)[..., None] * memory_state + inject[..., None] * value_pre[:, :, None, :]
    )
    readout = jnp.einsum(
        "bhk,bhkv->bhv", jax.nn.silu(query_pre), next_state, precision=lax.Precision.HIGHEST
    )
    normed = (
        readout
        * lax.rsqrt(jnp.mean(readout * readout, axis=2, keepdims=True) + EPSILON)
        * head_gain.reshape(local_heads, HEAD_DIM)
    )
    mixed_heads = (
        (normed * jax.nn.silu(outgate_pre))
        .reshape(seq_rows, local_heads * HEAD_DIM)
        .astype(jnp.bfloat16)
    )
    partial_out = jnp.dot(mixed_heads, out_weight, preferred_element_type=jnp.float32)
    mixed = sent_and_summed(partial_out.astype(jnp.bfloat16), "tp", 1)
    return (mixed, next_state)


def shards(
    residual_in,
    gain_pre,
    gate_pre,
    up_pre,
    down_pre,
    gain_mix,
    query_weight,
    forget_weight,
    value_weight,
    outgate_weight,
    lower_bound,
    head_gain,
    out_weight,
    gain_post,
    gate_post,
    up_post,
    down_post,
    memory_state,
):
    branch_a = channel_mixer(residual_in, gain_pre, gate_pre, up_pre, down_pre)
    stream_a = (residual_in.astype(jnp.float32) + 0.5 * branch_a).astype(jnp.bfloat16)
    mixed, next_state = token_mixer(
        stream_a,
        gain_mix,
        query_weight,
        forget_weight,
        value_weight,
        outgate_weight,
        lower_bound,
        head_gain,
        out_weight,
        memory_state,
    )
    stream_b = (stream_a.astype(jnp.float32) + mixed).astype(jnp.bfloat16)
    branch_b = channel_mixer(stream_b, gain_post, gate_post, up_post, down_post)
    layer_out = (stream_b.astype(jnp.float32) + 0.5 * branch_b).astype(jnp.bfloat16)
    return (layer_out, next_state)


def solution(mesh):
    in_specs = (
        P("kv", "tp"),
        P("tp"),
        P("tp", "kv"),
        P("tp", "kv"),
        P("kv", "tp"),
        P(),
        P("kv", "tp"),
        P("kv", "tp"),
        P("kv", "tp"),
        P("kv", "tp"),
        P("tp"),
        P("tp"),
        P("tp", None),
        P("tp"),
        P("tp", "kv"),
        P("tp", "kv"),
        P("kv", "tp"),
        P("kv", "tp", None, None),
    )
    out_specs = (P("kv", "tp"), P("kv", "tp", None, None))
    return jax.shard_map(shards, mesh=mesh, in_specs=in_specs, out_specs=out_specs, check_vma=False)
```

profile of v0, /device:TPU:1, one launch (start us, length us, event | category | flops | bytes accessed | tf_op | source)
XLA Modules:
  0.0 270.0 jit_solution(2445144380313913863)
XLA Ops:
  7.3 1.5 pad_maximum_fusion.2
  8.8 0.7 broadcast_in_dim.10
  9.5 39.3 %all_to_all.50 = bf16[64,6,256]{2,1,0:T(8,128)(2,1)S(1)} all-to-all(bf16[64,6,256]{2,1,0:T(8,128)(2,1)S(1)} %broadcast_in_dim.10), channel_id=1, replica_groups=mesh['kv'=64,'tp'=8] {'kv'}, dimensions={0} | all-to-all | bytes 393216 | tf_op jit(solution)/shard_map/all_to_all | solution.py:21
  49.2 1.0 convolution_convert_fusion.6
  50.3 1.0 convolution_convert_fusion.5
  51.6 13.7 %all_to_all.51 = bf16[8,48,177]{2,1,0:T(8,128)(2,1)S(1)} all-to-all(bf16[8,48,177]{2,1,0:T(8,128)(2,1)S(1)} %pad_maximum_fusion), channel_id=1, replica_groups=mesh['kv'=64,'tp'=8] {'tp'}, dimensions={0} | all-to-all | bytes 271872 | tf_op jit(solution)/shard_map/all_to_all | solution.py:36
  65.6 8.3 %all_to_all.52 = bf16[8,48,88]{2,1,0:T(8,128)(2,1)S(1)} all-to-all(bf16[8,48,88]{2,1,0:T(8,128)(2,1)S(1)} %broadcast_in_dim.11), channel_id=1, replica_groups=mesh['kv'=64,'tp'=8] {'tp'}, dimensions={0} | all-to-all | bytes 135168 | tf_op jit(solution)/shard_map/all_to_all | solution.py:21
  74.2 24.4 %all_to_all.53 = bf16[64,6,256]{2,1,0:T(8,128)(2,1)S(1)} all-to-all(bf16[64,6,256]{2,1,0:T(8,128)(2,1)S(1)} %reshape.206), channel_id=1, replica_groups=mesh['kv'=64,'tp'=8] {'kv'}, dimensions={0} | all-to-all | bytes 393216 | tf_op jit(solution)/shard_map/all_to_all | solution.py:36
  98.7 0.6 broadcast_in_dim.12
  99.3 6.9 %all-to-all-start.4 = ((bf16[8,6,256]{2,1,0:T(8,128)(2,1)}), bf16[8,6,256]{2,1,0:T(8,128)(2,1)S(1)}, u32[]{:S(2)}, u32[]{:S(2)}) async-start(bf16[8,6,256]{2,1,0:T(8,128)(2,1)} %broadcast_in_dim.12), calls=%async_computation.4 | async-start | bytes 65536 | tf_op jit(solution)/shard_map/all_to_all | solution.py:21
  106.3 4.8 %all-to-all-done.4 = bf16[8,6,256]{2,1,0:T(8,128)(2,1)S(1)} async-done(((bf16[8,6,256]{2,1,0:T(8,128)(2,1)}), bf16[8,6,256]{2,1,0:T(8,128)(2,1)S(1)}, u32[]{:S(2)}, u32[]{:S(2)}) %all-to-all-start.4) | async-done | bytes 24608 | tf_op jit(solution)/shard_map/all_to_all | solution.py:21
  111.2 44.6 %all-gather.2.cloned.1.call-done = bf16[2048,1024]{1,0:T(8,128)(2,1)} async-done(((bf16[32,1024]{1,0:T(8,128)(2,1)}), bf16[2048,1024]{1,0:T(8,128)(2,1)}) %all-gather.2.cloned.1.call-update) | async-done | bytes 4194320 | tf_op jit(solution)/shard_map/all_gather | solution.py:54
  155.9 3.9 %slice_bitcast_fusion.3 = (bf16[256,2048]{0,1:T(8,128)(2,1)S(1)}, bf16[256,2048]{0,1:T(8,128)(2,1)}, bf16[256,2048]{0,1:T(8,128)(2,1)}, bf16[256,2048]{0,1:T(8,128)(2,1)}) fusion(bf16[2048,1024]{1,0:T(8,128)(2,1)} %all-gather.2.cloned.1.call-done), kind=kLoop, calls=%fused_computation.14 | loop fusion | bytes 8388608 | tf_op jit(solution)/shard_map/dot_general | solution.py:107
  159.8 0.6 copy.61
  160.4 1.5 copy.64
  162.7 1.5 copy.63
  164.6 1.5 copy.62
  166.7 1.6 multiply_add_fusion
  168.3 0.8 fusion.22
  169.5 18.4 %all_to_all.54 = bf16[8,6,256]{2,1,0:T(8,128)(2,1)S(1)} all-to-all(bf16[8,6,256]{2,1,0:T(8,128)(2,1)S(1)} %bitcast.125), channel_id=1, replica_groups=mesh['kv'=64,'tp'=8] {'tp'}, dimensions={0} | all-to-all | bytes 49152 | tf_op jit(solution)/shard_map/all_to_all | solution.py:36
  188.0 28.2 %all_to_all.55 = bf16[64,6,256]{2,1,0:T(8,128)(2,1)S(1)} all-to-all(bf16[64,6,256]{2,1,0:T(8,128)(2,1)S(1)} %broadcast_in_dim.13), channel_id=1, replica_groups=mesh['kv'=64,'tp'=8] {'kv'}, dimensions={0} | all-to-all | bytes 393216 | tf_op jit(solution)/shard_map/all_to_all | solution.py:21
  217.4 12.2 %all_to_all.56 = bf16[8,48,177]{2,1,0:T(8,128)(2,1)S(1)} all-to-all(bf16[8,48,177]{2,1,0:T(8,128)(2,1)S(1)} %pad_maximum_fusion.1), channel_id=1, replica_groups=mesh['kv'=64,'tp'=8] {'tp'}, dimensions={0} | all-to-all | bytes 271872 | tf_op jit(solution)/shard_map/all_to_all | solution.py:36
  230.0 8.3 %all_to_all.57 = bf16[8,48,88]{2,1,0:T(8,128)(2,1)S(1)} all-to-all(bf16[8,48,88]{2,1,0:T(8,128)(2,1)S(1)} %broadcast_in_dim.14), channel_id=1, replica_groups=mesh['kv'=64,'tp'=8] {'tp'}, dimensions={0} | all-to-all | bytes 135168 | tf_op jit(solution)/shard_map/all_to_all | solution.py:21
  238.6 23.9 %all_to_all.58 = bf16[64,6,256]{2,1,0:T(8,128)(2,1)S(1)} all-to-all(bf16[64,6,256]{2,1,0:T(8,128)(2,1)S(1)} %reshape.213), channel_id=1, replica_groups=mesh['kv'=64,'tp'=8] {'kv'}, dimensions={0} | all-to-all | bytes 393216 | tf_op jit(solution)/shard_map/all_to_all | solution.py:36
  (74 shorter events, 6.2 us)
Async XLA Ops:
  7.2 162.0 %copy-start = (bf16[256,2048]{1,0:T(8,128)(2,1)S(1)}, bf16[256,2048]{1,0:T(8,128)(2,1)}, u32[]{:S(2)}) copy-start(bf16[256,2048]{1,0:T(8,128)(2,1)} %param.30) | copy-start | bytes 3145732
  7.2 91.5 %copy-start.6 = (bf16[6,256]{1,0:T(8,128)(2,1)S(1)}, bf16[6,256]{1,0:T(8,128)(2,1)}, u32[]{:S(2)}) copy-start(bf16[6,256]{1,0:T(8,128)(2,1)} %param.18) | copy-start | bytes 9220
  7.2 66.7 %copy-start.2 = (bf16[88,256]{1,0:T(8,128)(2,1)S(1)}, bf16[88,256]{1,0:T(8,128)(2,1)}, u32[]{:S(2)}) copy-start(bf16[88,256]{1,0:T(8,128)(2,1)} %param.22) | copy-start | bytes 135172
  7.2 99.1 %copy-start.9 = (f32[256]{0:T(256)S(1)}, f32[256]{0:T(256)}, u32[]{:S(2)}) copy-start(f32[256]{0:T(256)} %param.28) | copy-start | bytes 3076
  7.2 99.1 %copy-start.7 = (f32[2048]{0:T(1024)S(1)}, f32[2048]{0:T(1024)}, u32[]{:S(2)}) copy-start(f32[2048]{0:T(1024)} %param.23) | copy-start | bytes 24580
  7.2 148.6 %all-gather.2.cloned.1.call-start = ((), (), s32[]{:S(2)}) async-start(), calls=%async_computation.10 | async-start | bytes 4259840 | tf_op jit(solution)/shard_map/all_gather | solution.py:54
  99.3 11.7 %all-to-all-start.4 = ((bf16[8,6,256]{2,1,0:T(8,128)(2,1)}), bf16[8,6,256]{2,1,0:T(8,128)(2,1)S(1)}, u32[]{:S(2)}, u32[]{:S(2)}) async-start(bf16[8,6,256]{2,1,0:T(8,128)(2,1)} %broadcast_in_dim.12), calls=%async_computation.4 | async-start | bytes 65536 | tf_op jit(solution)/shard_map/all_to_all | solution.py:21
  162.7 6.5 %copy-start.10 = (f32[256]{0:T(256)S(1)}, f32[256]{0:T(256)}, u32[]{:S(2)}) copy-start(f32[256]{0:T(256)} %param.29) | copy-start | bytes 3076
  164.6 52.0 %copy-start.4 = (bf16[256,88]{0,1:T(8,128)(2,1)S(1)}, bf16[256,88]{0,1:T(8,128)(2,1)}, u32[]{:S(2)}) copy-start(bf16[256,88]{0,1:T(8,128)(2,1)} %param.33) | copy-start | bytes 135172
  164.6 52.0 %copy-start.8 = (f32[256]{0:T(256)S(1)}, f32[256]{0:T(256)}, u32[]{:S(2)}) copy-start(f32[256]{0:T(256)} %param.31) | copy-start | bytes 3076
  164.6 52.2 %copy-start.5 = (bf16[256,88]{0,1:T(8,128)(2,1)S(1)}, bf16[256,88]{0,1:T(8,128)(2,1)}, u32[]{:S(2)}) copy-start(bf16[256,88]{0,1:T(8,128)(2,1)} %param.32) | copy-start | bytes 135172
  166.7 71.6 %copy-start.3 = (bf16[88,256]{1,0:T(8,128)(2,1)S(1)}, bf16[88,256]{1,0:T(8,128)(2,1)}, u32[]{:S(2)}) copy-start(bf16[88,256]{1,0:T(8,128)(2,1)} %param.34) | copy-start | bytes 135172
  168.3 94.9 %copy-start.1 = (f32[6,2,128,128]{3,2,1,0:T(8,128)}, f32[6,2,128,128]{3,2,1,0:T(8,128)S(1)}, u32[]{:S(2)}) copy-start(f32[6,2,128,128]{3,2,1,0:T(8,128)S(1)} %multiply_add_fusion) | copy-start | bytes 2359300
Sparse Core Ops, SparseCore 0:
  11.5 144.2 all-gather.1
where the time goes:
time: 272 us; the launch traced here: 270 us
  blocking collectives  177 us (65%)
  waiting for transfers between devices  49.4 us (18%)
  between operations  14.4 us (5%)
  local copies, waits for them, and re-layouts  11.6 us (4%)
  starting transfers between devices  6.97 us (3%)
  other arithmetic  5.51 us (2%)
  matrix products  5.34 us (2%)
    all_to_all x5, blocking collectives, sent_and_summed(): lax.all_to_all(tiles, axis, split_axis=0, concat_axis=0, tiled=True)  92.7 us
    all_to_all x4, blocking collectives, sent_to_all(): return lax.all_to_all(copies, axis, split_axis=0, concat_axis=0, tiled=True)  84.1 us
    all_gather x1, waiting for transfers between devices, in_one_piece(): filled = lax.all_gather(both, axis, axis=dim, tiled=True)  44.6 us
    dot_general x5, local copies, waits for them, and re-layouts, token_mixer(): jnp.dot(scaled, weight_rows, preferred_element_type=jnp.float32)  9.11 us
    all_to_all x1, starting transfers between devices, sent_to_all(): return lax.all_to_all(copies, axis, split_axis=0, concat_axis=0, tiled=True)  6.93 us
  transfers between devices with their start and end apart: 2, of which 2 were waited for; matrix products, arithmetic and copies ran while one was open for 2% of the time, Pallas kernels for 0%

commit v1 on v0

v1 whole, which is shorter than its diff:
```python
import jax
import jax.numpy as jnp
from jax import lax
from jax.sharding import Mesh, PartitionSpec as P

D = 2048
HEAD_DIM = 128
EPSILON = 1e-06
TP = ("x", "c")

f32 = jnp.float32
bf16 = jnp.bfloat16


def exchanged(tiles, axis):
    return lax.all_to_all(tiles, axis, split_axis=0, concat_axis=0, tiled=True)


def gathered(array, axis):
    return exchanged(jnp.broadcast_to(array, (lax.axis_size(axis), *array.shape)), axis)


def dot(a, b, da, db):
    return lax.dot_general(a, b, (((da,), (db,)), ((), ())), preferred_element_type=f32)


def padded(array, rows):
    return jnp.pad(array, ((0, rows - array.shape[0]), (0, 0)))


def hidden_units(rows, gain_vec, gate_t, up_t, extra):
    tp = lax.axis_size(TP)
    n = rows.shape[0]
    widened = rows.astype(f32)
    squares = jnp.sum(widened * widened, axis=1)
    scaled = (widened * gain_vec).astype(bf16)
    gate_part = dot(gate_t, scaled, 1, 1).astype(bf16)
    up_part = dot(up_t, scaled, 1, 1).astype(bf16)
    unit = gate_part.shape[0] // tp
    tiles = [
        gate_part.reshape(tp, unit, n),
        up_part.reshape(tp, unit, n),
        jnp.broadcast_to(squares.astype(bf16), (tp, 8, n)),
    ]
    if extra is not None:
        tiles.append(extra)
    arrived = exchanged(jnp.concatenate(tiles, axis=1), TP)
    summed = arrived[:, : 2 * unit + 8].astype(f32).sum(axis=0)
    inverse = lax.rsqrt(summed[2 * unit] / D + EPSILON)[None, :]
    hidden = (jax.nn.silu(summed[:unit] * inverse) * (summed[unit : 2 * unit] * inverse)).astype(bf16)
    every = gathered(hidden, TP).reshape(tp * unit, n)
    return every, arrived[:, 2 * unit + 8 :]


def shards(
    residual_in,
    gain_pre,
    gate_pre,
    up_pre,
    down_pre,
    gain_mix,
    query_weight,
    forget_weight,
    value_weight,
    outgate_weight,
    lower_bound,
    head_gain,
    out_weight,
    gain_post,
    gate_post,
    up_post,
    down_post,
    memory_state,
):
    nz, ny, tp = lax.axis_size("z"), lax.axis_size("y"), lax.axis_size(TP)
    z_at, t_at = lax.axis_index("z"), lax.axis_index(TP)
    own, width = residual_in.shape
    rows = nz * own
    units = gate_pre.shape[1]
    unit = -(-units * ny // (8 * tp)) * 8 * tp // ny
    block = width * tp // nz
    piece = block // tp
    halves = width // block

    first = jnp.concatenate([padded(gate_pre.T, unit), padded(up_pre.T, unit)], axis=0)
    first = gathered(first, "y")
    gate_pre_t = first[:, :unit].reshape(ny * unit, width)
    up_pre_t = first[:, unit:].reshape(ny * unit, width)

    down_t = down_pre.T.reshape(halves, tp, piece, units).swapaxes(0, 1)
    down_t = exchanged(down_t.reshape(tp, halves * piece, units), TP).reshape(width, units)
    kept = query_weight.shape[0]
    second = jnp.concatenate(
        [
            padded(down_t.T, unit),
            padded(gate_post.T, unit),
            padded(up_post.T, unit),
            padded(down_post, unit),
            query_weight,
            forget_weight,
            value_weight,
            outgate_weight,
        ],
        axis=0,
    )
    second = gathered(second, "y")
    down_pre_all, gate_post_t, up_post_t, down_post_all = (
        second[:, k * unit : (k + 1) * unit].reshape(ny * unit, width) for k in range(4)
    )
    mixers = [
        second[:, 4 * unit + k * kept : 4 * unit + (k + 1) * kept].reshape(ny * kept, width)
        for k in range(4)
    ]

    all_rows = gathered(residual_in, "z").reshape(rows, width)
    turned = all_rows.T.reshape(halves, tp, piece, rows).swapaxes(0, 1)
    hidden, residual = hidden_units(
        all_rows, gain_pre, gate_pre_t, up_pre_t, turned.reshape(tp, halves * piece, rows)
    )
    residual = lax.dynamic_index_in_dim(
        residual.reshape(nz, piece, rows), z_at, axis=0, keepdims=False
    )
    part = dot(down_pre_all, hidden, 0, 0).astype(bf16)
    branch = exchanged(part.reshape(nz, piece, rows), "z").astype(f32).sum(axis=0)
    stream_piece = (residual.astype(f32) + 0.5 * branch).astype(bf16)

    stream_t = gathered(stream_piece, TP).reshape(block, rows)
    widened = stream_t.astype(f32)
    squares = jnp.sum(widened * widened, axis=0)
    gain_block = lax.dynamic_slice_in_dim(gain_mix, z_at * block, block)
    scaled = (widened * gain_block[:, None]).astype(bf16)
    parts = [dot(scaled, weight, 0, 0).astype(bf16).reshape(nz, own, width) for weight in mixers]
    mine = z_at // halves == t_at
    note = jnp.where(
        mine,
        stream_t.T.reshape(nz, own, block),
        jnp.broadcast_to(squares.astype(bf16).reshape(nz, own, 1), (nz, own, block)),
    )
    arrived = exchanged(jnp.concatenate([*parts, note], axis=2), "z")
    projected = arrived[:, :, : 4 * width].astype(f32).sum(axis=0)
    notes = arrived[:, :, 4 * width :]
    stream_a = lax.dynamic_slice_in_dim(notes, t_at * halves, halves, axis=0)
    stream_a = stream_a.swapaxes(0, 1).reshape(own, width).astype(f32)
    elsewhere = (jnp.arange(nz) // halves != t_at)[:, None]
    total = jnp.sum(jnp.where(elsewhere, notes[:, :, 0].astype(f32), 0.0), axis=0)
    total = total + jnp.sum(stream_a * stream_a, axis=1)
    projected = projected * lax.rsqrt(total / D + EPSILON)[:, None]

    heads = width // HEAD_DIM
    query_pre, forget_pre, value_pre, outgate_pre = (
        projected[:, k * width : (k + 1) * width].reshape(own, heads, HEAD_DIM) for k in range(4)
    )
    floor_rate = lower_bound.reshape(heads, HEAD_DIM)
    log_keep = jnp.logaddexp(
        jnp.log(floor_rate), jnp.log1p(-floor_rate) + jax.nn.log_sigmoid(forget_pre)
    )
    inject = (1.0 - floor_rate) * jax.nn.sigmoid(-forget_pre)
    next_state = (
        jnp.exp(log_keep)[..., None] * memory_state + inject[..., None] * value_pre[:, :, None, :]
    )
    readout = jnp.einsum(
        "bhk,bhkv->bhv", jax.nn.silu(query_pre), next_state, precision=lax.Precision.HIGHEST
    )
    normed = (
        readout
        * lax.rsqrt(jnp.mean(readout * readout, axis=2, keepdims=True) + EPSILON)
        * head_gain.reshape(heads, HEAD_DIM)
    )
    mixed_heads = (normed * jax.nn.silu(outgate_pre)).reshape(own, width).astype(bf16)
    partial_out = dot(mixed_heads, out_weight, 1, 0).astype(bf16)
    mixed = exchanged(partial_out.reshape(own, tp, width).swapaxes(0, 1), TP)
    stream_b = (stream_a + mixed.astype(f32).sum(axis=0)).astype(bf16)

    all_rows = gathered(stream_b, "z").reshape(rows, width)
    hidden, _ = hidden_units(all_rows, gain_post, gate_post_t, up_post_t, None)
    part = dot(hidden, down_post_all, 0, 0).astype(bf16)
    branch = exchanged(part.reshape(nz, own, width), "z").astype(f32).sum(axis=0)
    layer_out = (stream_b.astype(f32) + 0.5 * branch).astype(bf16)
    return (layer_out, next_state)


def solution(mesh):
    grid = Mesh(mesh.devices.reshape(16, 4, 4, 2), ("z", "y", "x", "c"))
    kv = ("z", "y")
    in_specs = (
        P(kv, TP),
        P(TP),
        P(TP, kv),
        P(TP, kv),
        P(kv, TP),
        P(),
        P(kv, TP),
        P(kv, TP),
        P(kv, TP),
        P(kv, TP),
        P(TP),
        P(TP),
        P(TP, None),
        P(TP),
        P(TP, kv),
        P(TP, kv),
        P(kv, TP),
        P(kv, TP, None, None),
    )
    out_specs = (P(kv, TP), P(kv, TP, None, None))
    return jax.shard_map(shards, mesh=grid, in_specs=in_specs, out_specs=out_specs, check_vma=False)
```

time: 272 us -> 213 us (0.78)
  blocking collectives: 177 us -> 63.4 us
  starting transfers between devices: 6.97 us -> 53.1 us
  waiting for transfers between devices: 49.4 us -> 68.8 us
  between operations: 14.4 us -> 1.22 us
  local copies, waits for them, and re-layouts: 11.6 us -> 18.6 us
    all_to_all x9 -> x5, blocking collectives: 177 us -> 63.4 us  [exchanged(): return lax.all_to_all(tiles, axis, split_axis=0, concat_axis=0, tiled=True)]
    all_to_all x1 -> x9, waiting for transfers between devices: 4.76 us -> 68.8 us  [exchanged(): return lax.all_to_all(tiles, axis, split_axis=0, concat_axis=0, tiled=True)]
    all_to_all x1 -> x9, starting transfers between devices: 6.93 us -> 53.1 us  [exchanged(): return lax.all_to_all(tiles, axis, split_axis=0, concat_axis=0, tiled=True)]
    all_gather x1 -> x0, waiting for transfers between devices: 44.6 us -> none  [in_one_piece(): filled = lax.all_gather(both, axis, axis=dim, tiled=True)]
    dot_general x5 -> x0, local copies, waits for them, and re-layouts: 9.11 us -> none  [token_mixer(): jnp.dot(scaled, weight_rows, preferred_element_type=jnp.float32)]
    unnamed x22 -> x54, local copies, waits for them, and re-layouts: 0.07 us -> 9.13 us
    broadcast_in_dim x5 -> x9, local copies, waits for them, and re-layouts: 1.36 us -> 4.54 us  [the longest x7 4.53 us: gathered(): jnp.broadcast_to(array, (lax.axis_size(axis), *array.shape))]
  transfers between devices with their start and end apart: 2 -> 9, of which waited for: 2 -> 9; matrix products, arithmetic and copies ran while one was open for 2% -> 3% of each run, Pallas kernels for 0% -> 0%
where the time goes in v1:
time: 213 us; the launch traced here: 212 us
  waiting for transfers between devices  68.8 us (32%)
  blocking collectives  63.4 us (30%)
  starting transfers between devices  53.1 us (25%)
  local copies, waits for them, and re-layouts  18.6 us (9%)
  other arithmetic  3.88 us (2%)
  matrix products  2.98 us (1%)
    all_to_all x9, waiting for transfers between devices, exchanged(): return lax.all_to_all(tiles, axis, split_axis=0, concat_axis=0, tiled=True)  68.8 us
    all_to_all x5, blocking collectives, exchanged(): return lax.all_to_all(tiles, axis, split_axis=0, concat_axis=0, tiled=True)  63.4 us
    all_to_all x9, starting transfers between devices, exchanged(): return lax.all_to_all(tiles, axis, split_axis=0, concat_axis=0, tiled=True)  53.1 us
    unnamed x54, local copies, waits for them, and re-layouts  9.13 us
    broadcast_in_dim x7, local copies, waits for them, and re-layouts, gathered(): jnp.broadcast_to(array, (lax.axis_size(axis), *array.shape))  4.53 us
  transfers between devices with their start and end apart: 9, of which 9 were waited for; matrix products, arithmetic and copies ran while one was open for 3% of the time, Pallas kernels for 0%

profile of v1, /device:TPU:1, one launch (start us, length us, event | category | flops | bytes accessed | tf_op | source)
XLA Modules:
  0.0 212.0 jit_solution(7192823086796233621)
XLA Ops:
  0.6 1.4 broadcast_in_dim.58
  2.1 15.9 %all-to-all-start.1 = ((bf16[16,6,256]{2,1,0:T(8,128)(2,1)}), bf16[16,6,256]{2,1,0:T(8,128)(2,1)S(1)}, u32[]{:S(2)}, u32[]{:S(2)}) async-start(bf16[16,6,256]{2,1,0:T(8,128)(2,1)} %broadcast_in_dim.58), calls=%async_computation.1 | async-start | bytes 131072 | tf_op jit(solution)/shard_map/all_to_all | solution.py:16
  18.0 11.5 %all-to-all-done.1 = bf16[16,6,256]{2,1,0:T(8,128)(2,1)S(1)} async-done(((bf16[16,6,256]{2,1,0:T(8,128)(2,1)}), bf16[16,6,256]{2,1,0:T(8,128)(2,1)S(1)}, u32[]{:S(2)}, u32[]{:S(2)}) %all-to-all-start.1) | async-done | bytes 49184 | tf_op jit(solution)/shard_map/all_to_all | solution.py:16
  30.3 4.3 %all-to-all-start = ((bf16[4,192,256]{2,1,0:T(8,128)(2,1)}), bf16[4,192,256]{2,1,0:T(8,128)(2,1)S(1)}, u32[]{:S(2)}, u32[]{:S(2)}) async-start(bf16[4,192,256]{2,1,0:T(8,128)(2,1)} %broadcast_in_dim.32), calls=%async_computation | async-start | bytes 786432 | tf_op jit(solution)/shard_map/all_to_all | solution.py:16
  35.8 5.0 %all-to-all-done = bf16[4,192,256]{2,1,0:T(8,128)(2,1)S(1)} async-done(((bf16[4,192,256]{2,1,0:T(8,128)(2,1)}), bf16[4,192,256]{2,1,0:T(8,128)(2,1)S(1)}, u32[]{:S(2)}, u32[]{:S(2)}) %all-to-all-start) | async-done | bytes 393248 | tf_op jit(solution)/shard_map/all_to_all | solution.py:16
  40.8 7.8 %all-to-all-start.3 = ((bf16[8,32,88]{2,1,0:T(8,128)(2,1)}), bf16[8,32,88]{2,1,0:T(8,128)(2,1)S(1)}, u32[]{:S(2)}, u32[]{:S(2)}) async-start(bf16[8,32,88]{2,1,0:T(8,128)(2,1)} %bitcast.15), calls=%async_computation.3 | async-start | bytes 131072 | tf_op jit(solution)/shard_map/all_to_all | solution.py:16
  50.2 3.4 %all-to-all-done.3 = bf16[8,32,88]{2,1,0:T(8,128)(2,1)S(1)} async-done(((bf16[8,32,88]{2,1,0:T(8,128)(2,1)}), bf16[8,32,88]{2,1,0:T(8,128)(2,1)S(1)}, u32[]{:S(2)}, u32[]{:S(2)}) %all-to-all-start.3) | async-done | bytes 45088 | tf_op jit(solution)/shard_map/all_to_all | solution.py:16
  53.5 4.1 %all-to-all-start.2 = ((bf16[8,136,96]{2,1,0:T(8,128)(2,1)}), bf16[8,136,96]{2,1,0:T(8,128)(2,1)S(1)}, u32[]{:S(2)}, u32[]{:S(2)}) async-start(bf16[8,136,96]{2,1,0:T(8,128)(2,1)} %pad_maximum_fusion), calls=%async_computation.2 | async-start | bytes 557056 | tf_op jit(solution)/shard_map/all_to_all | solution.py:16
  62.8 1.4 all-to-all-done.2
  65.3 3.5 %all-to-all-start.4 = ((bf16[4,512,256]{2,1,0:T(8,128)(2,1)}), bf16[4,512,256]{2,1,0:T(8,128)(2,1)S(1)}, u32[]{:S(2)}, u32[]{:S(2)}) async-start(bf16[4,512,256]{2,1,0:T(8,128)(2,1)} %broadcast_in_dim.60), calls=%async_computation.4 | async-start | bytes 2097152 | tf_op jit(solution)/shard_map/all_to_all | solution.py:16
  68.9 14.0 %all-to-all-done.4 = bf16[4,512,256]{2,1,0:T(8,128)(2,1)S(1)} async-done(((bf16[4,512,256]{2,1,0:T(8,128)(2,1)}), bf16[4,512,256]{2,1,0:T(8,128)(2,1)S(1)}, u32[]{:S(2)}, u32[]{:S(2)}) %all-to-all-start.4) | async-done | bytes 1048608 | tf_op jit(solution)/shard_map/all_to_all | solution.py:16
  83.6 5.2 %all-to-all-start.5 = ((bf16[8,48,96]{2,1,0:T(8,128)(2,1)}), bf16[8,48,96]{2,1,0:T(8,128)(2,1)S(1)}, u32[]{:S(2)}, u32[]{:S(2)}) async-start(bf16[8,48,96]{2,1,0:T(8,128)(2,1)} %broadcast_in_dim.61), calls=%async_computation.5 | async-start | bytes 196608 | tf_op jit(solution)/shard_map/all_to_all | solution.py:16
  89.5 4.3 %all-to-all-done.5 = bf16[8,48,96]{2,1,0:T(8,128)(2,1)S(1)} async-done(((bf16[8,48,96]{2,1,0:T(8,128)(2,1)}), bf16[8,48,96]{2,1,0:T(8,128)(2,1)S(1)}, u32[]{:S(2)}, u32[]{:S(2)}) %all-to-all-start.5) | async-done | bytes 73760 | tf_op jit(solution)/shard_map/all_to_all | solution.py:16
  94.7 3.5 %all-to-all-start.6 = ((bf16[16,16,96]{2,1,0:T(8,128)(2,1)}), bf16[16,16,96]{2,1,0:T(8,128)(2,1)S(1)}, u32[]{:S(2)}, u32[]{:S(2)}) async-start(bf16[16,16,96]{2,1,0:T(8,128)(2,1)} %bitcast.23), calls=%async_computation.6 | async-start | bytes 131072 | tf_op jit(solution)/shard_map/all_to_all | solution.py:16
  99.1 10.8 %all-to-all-done.6 = bf16[16,16,96]{2,1,0:T(8,128)(2,1)S(1)} async-done(((bf16[16,16,96]{2,1,0:T(8,128)(2,1)}), bf16[16,16,96]{2,1,0:T(8,128)(2,1)S(1)}, u32[]{:S(2)}, u32[]{:S(2)}) %all-to-all-start.6) | async-done | bytes 49184 | tf_op jit(solution)/shard_map/all_to_all | solution.py:16
  110.5 5.3 %all-to-all-start.7 = ((bf16[8,16,96]{2,1,0:T(8,128)(2,1)}), bf16[8,16,96]{2,1,0:T(8,128)(2,1)S(1)}, u32[]{:S(2)}, u32[]{:S(2)}) async-start(bf16[8,16,96]{2,1,0:T(8,128)(2,1)} %broadcast_in_dim.62), calls=%async_computation.7 | async-start | bytes 65536 | tf_op jit(solution)/shard_map/all_to_all | solution.py:16
  115.8 4.7 %all-to-all-done.7 = bf16[8,16,96]{2,1,0:T(8,128)(2,1)S(1)} async-done(((bf16[8,16,96]{2,1,0:T(8,128)(2,1)}), bf16[8,16,96]{2,1,0:T(8,128)(2,1)S(1)}, u32[]{:S(2)}, u32[]{:S(2)}) %all-to-all-start.7) | async-done | bytes 24608 | tf_op jit(solution)/shard_map/all_to_all | solution.py:16
  125.0 3.5 %all-to-all-start.8 = ((bf16[16,6,1152]{2,1,0:T(8,128)(2,1)}), bf16[16,6,1152]{2,1,0:T(8,128)(2,1)S(1)}, u32[]{:S(2)}, u32[]{:S(2)}) async-start(bf16[16,6,1152]{2,1,0:T(8,128)(2,1)} %select_dynamic-update-slice_fusion), calls=%async_computation.8 | async-start | bytes 589824 | tf_op jit(solution)/shard_map/all_to_all | solution.py:16
  129.2 13.6 %all-to-all-done.8 = bf16[16,6,1152]{2,1,0:T(8,128)(2,1)S(1)} async-done(((bf16[16,6,1152]{2,1,0:T(8,128)(2,1)}), bf16[16,6,1152]{2,1,0:T(8,128)(2,1)S(1)}, u32[]{:S(2)}, u32[]{:S(2)}) %all-to-all-start.8) | async-done | bytes 221216 | tf_op jit(solution)/shard_map/all_to_all | solution.py:16
  145.9 13.3 %all_to_all.70 = bf16[8,6,256]{2,1,0:T(8,128)(2,1)S(1)} all-to-all(bf16[8,6,256]{2,1,0:T(8,128)(2,1)S(1)} %bitcast.130), channel_id=1, replica_groups=mesh['z'=16,'y'=4,'x'=4,'c'=2] {'x','c'}, dimensions={0} | all-to-all | bytes 49152 | tf_op jit(solution)/shard_map/all_to_all | solution.py:16
  159.3 17.0 %all_to_all.71 = bf16[16,6,256]{2,1,0:T(8,128)(2,1)S(1)} all-to-all(bf16[16,6,256]{2,1,0:T(8,128)(2,1)S(1)} %broadcast_in_dim.66), channel_id=1, replica_groups=mesh['z'=16,'y'=4,'x'=4,'c'=2] {'z'}, dimensions={0} | all-to-all | bytes 98304 | tf_op jit(solution)/shard_map/all_to_all | solution.py:16
  177.4 10.4 %all_to_all.72 = bf16[8,104,96]{1,2,0:T(8,128)(2,1)S(1)} all-to-all(bf16[8,104,96]{1,2,0:T(8,128)(2,1)S(1)} %copy.236), channel_id=1, replica_groups=mesh['z'=16,'y'=4,'x'=4,'c'=2] {'x','c'}, dimensions={0} | all-to-all | bytes 319488 | tf_op jit(solution)/shard_map/all_to_all | solution.py:16
  188.4 8.4 %all_to_all.73 = bf16[8,48,96]{2,1,0:T(8,128)(2,1)S(1)} all-to-all(bf16[8,48,96]{2,1,0:T(8,128)(2,1)S(1)} %broadcast_in_dim.68), channel_id=1, replica_groups=mesh['z'=16,'y'=4,'x'=4,'c'=2] {'x','c'}, dimensions={0} | all-to-all | bytes 147456 | tf_op jit(solution)/shard_map/all_to_all | solution.py:16
  197.1 14.3 %all_to_all.74 = bf16[16,6,256]{2,1,0:T(8,128)(2,1)S(1)} all-to-all(bf16[16,6,256]{2,1,0:T(8,128)(2,1)S(1)} %reshape.301), channel_id=1, replica_groups=mesh['z'=16,'y'=4,'x'=4,'c'=2] {'z'}, dimensions={0} | all-to-all | bytes 98304 | tf_op jit(solution)/shard_map/all_to_all | solution.py:16
  (150 shorter events, 24.0 us)
Async XLA Ops:
  0.6 145.1 %copy-start = (bf16[256,2048]{1,0:T(8,128)(2,1)S(1)}, bf16[256,2048]{1,0:T(8,128)(2,1)}, u32[]{:S(2)}) copy-start(bf16[256,2048]{1,0:T(8,128)(2,1)} %param.30) | copy-start | bytes 3145732
  2.1 15.9 %copy-start.9 = (bf16[256,88]{0,1:T(8,128)(2,1)S(1)}, bf16[256,88]{0,1:T(8,128)(2,1)}, u32[]{:S(2)}) copy-start(bf16[256,88]{0,1:T(8,128)(2,1)} %param.21) | copy-start | bytes 135172
  2.1 15.9 %copy-start.10 = (bf16[256,88]{0,1:T(8,128)(2,1)S(1)}, bf16[256,88]{0,1:T(8,128)(2,1)}, u32[]{:S(2)}) copy-start(bf16[256,88]{0,1:T(8,128)(2,1)} %param.20) | copy-start | bytes 135172
  2.1 27.4 %all-to-all-start.1 = ((bf16[16,6,256]{2,1,0:T(8,128)(2,1)}), bf16[16,6,256]{2,1,0:T(8,128)(2,1)S(1)}, u32[]{:S(2)}, u32[]{:S(2)}) async-start(bf16[16,6,256]{2,1,0:T(8,128)(2,1)} %broadcast_in_dim.58), calls=%async_computation.1 | async-start | bytes 131072 | tf_op jit(solution)/shard_map/all_to_all | solution.py:16
  30.3 4.3 %copy-start.5 = (bf16[88,256]{1,0:T(8,128)(2,1)S(1)}, bf16[88,256]{1,0:T(8,128)(2,1)}, u32[]{:S(2)}) copy-start(bf16[88,256]{1,0:T(8,128)(2,1)} %param.22) | copy-start | bytes 135172
  30.3 10.5 %all-to-all-start = ((bf16[4,192,256]{2,1,0:T(8,128)(2,1)}), bf16[4,192,256]{2,1,0:T(8,128)(2,1)S(1)}, u32[]{:S(2)}, u32[]{:S(2)}) async-start(bf16[4,192,256]{2,1,0:T(8,128)(2,1)} %broadcast_in_dim.32), calls=%async_computation | async-start | bytes 786432 | tf_op jit(solution)/shard_map/all_to_all | solution.py:16
  40.8 12.7 %all-to-all-start.3 = ((bf16[8,32,88]{2,1,0:T(8,128)(2,1)}), bf16[8,32,88]{2,1,0:T(8,128)(2,1)S(1)}, u32[]{:S(2)}, u32[]{:S(2)}) async-start(bf16[8,32,88]{2,1,0:T(8,128)(2,1)} %bitcast.15), calls=%async_computation.3 | async-start | bytes 131072 | tf_op jit(solution)/shard_map/all_to_all | solution.py:16
  50.1 7.5 %copy-start.11 = (bf16[32,256]{1,0:T(8,128)(2,1)S(1)}, bf16[32,256]{1,0:T(8,128)(2,1)}, u32[]{:S(2)}) copy-start(bf16[32,256]{1,0:T(8,128)(2,1)} %param.24) | copy-start | bytes 49156
  53.5 10.7 %all-to-all-start.2 = ((bf16[8,136,96]{2,1,0:T(8,128)(2,1)}), bf16[8,136,96]{2,1,0:T(8,128)(2,1)S(1)}, u32[]{:S(2)}, u32[]{:S(2)}) async-start(bf16[8,136,96]{2,1,0:T(8,128)(2,1)} %pad_maximum_fusion), calls=%async_computation.2 | async-start | bytes 557056 | tf_op jit(solution)/shard_map/all_to_all | solution.py:16
  57.6 0.7 copy-start.12
  59.8 0.8 copy-start.6
  60.6 0.8 copy-start.7
  61.5 0.8 copy-start.8
  64.3 34.8 %copy-start.2 = (bf16[8,136,96]{2,1,0:T(8,128)(2,1)}, bf16[8,136,96]{2,1,0:T(8,128)(2,1)S(1)}, u32[]{:S(2)}) copy-start(bf16[8,136,96]{2,1,0:T(8,128)(2,1)S(1)} %all-to-all-done.2) | copy-start | bytes 626692
  65.3 17.6 %all-to-all-start.4 = ((bf16[4,512,256]{2,1,0:T(8,128)(2,1)}), bf16[4,512,256]{2,1,0:T(8,128)(2,1)S(1)}, u32[]{:S(2)}, u32[]{:S(2)}) async-start(bf16[4,512,256]{2,1,0:T(8,128)(2,1)} %broadcast_in_dim.60), calls=%async_computation.4 | async-start | bytes 2097152 | tf_op jit(solution)/shard_map/all_to_all | solution.py:16
  83.6 10.2 %all-to-all-start.5 = ((bf16[8,48,96]{2,1,0:T(8,128)(2,1)}), bf16[8,48,96]{2,1,0:T(8,128)(2,1)S(1)}, u32[]{:S(2)}, u32[]{:S(2)}) async-start(bf16[8,48,96]{2,1,0:T(8,128)(2,1)} %broadcast_in_dim.61), calls=%async_computation.5 | async-start | bytes 196608 | tf_op jit(solution)/shard_map/all_to_all | solution.py:16
  94.7 15.1 %all-to-all-start.6 = ((bf16[16,16,96]{2,1,0:T(8,128)(2,1)}), bf16[16,16,96]{2,1,0:T(8,128)(2,1)S(1)}, u32[]{:S(2)}, u32[]{:S(2)}) async-start(bf16[16,16,96]{2,1,0:T(8,128)(2,1)} %bitcast.23), calls=%async_computation.6 | async-start | bytes 131072 | tf_op jit(solution)/shard_map/all_to_all | solution.py:16
  99.1 10.8 %slice-start = ((bf16[8,136,96]{2,1,0:T(8,128)(2,1)}), bf16[8,32,96]{2,1,0:T(8,128)(2,1)S(1)}, s32[]{:S(2)}) async-start(bf16[8,136,96]{2,1,0:T(8,128)(2,1)} %copy-done.2), calls=%async_computation.14 | async-start | bytes 131072 | tf_op jit(solution)/shard_map/slice | solution.py:52
  110.5 10.0 %all-to-all-start.7 = ((bf16[8,16,96]{2,1,0:T(8,128)(2,1)}), bf16[8,16,96]{2,1,0:T(8,128)(2,1)S(1)}, u32[]{:S(2)}, u32[]{:S(2)}) async-start(bf16[8,16,96]{2,1,0:T(8,128)(2,1)} %broadcast_in_dim.62), calls=%async_computation.7 | async-start | bytes 65536 | tf_op jit(solution)/shard_map/all_to_all | solution.py:16
  123.7 19.9 %copy-start.3 = (f32[6,2,128,128]{3,2,1,0:T(8,128)S(1)}, f32[6,2,128,128]{3,2,1,0:T(8,128)}, u32[]{:S(2)}) copy-start(f32[6,2,128,128]{3,2,1,0:T(8,128)} %param.35) | copy-start | bytes 2359300
  125.0 17.9 %all-to-all-start.8 = ((bf16[16,6,1152]{2,1,0:T(8,128)(2,1)}), bf16[16,6,1152]{2,1,0:T(8,128)(2,1)S(1)}, u32[]{:S(2)}, u32[]{:S(2)}) async-start(bf16[16,6,1152]{2,1,0:T(8,128)(2,1)} %select_dynamic-update-slice_fusion), calls=%async_computation.8 | async-start | bytes 589824 | tf_op jit(solution)/shard_map/all_to_all | solution.py:16
  144.1 1.9 copy-start.1
  159.3 17.0 %copy-start.16 = (f32[256]{0:T(256)S(1)}, f32[256]{0:T(256)}, u32[]{:S(2)}) copy-start(f32[256]{0:T(256)} %param.31) | copy-start | bytes 3076
  188.3 8.5 %copy-start.4 = (bf16[4,96,256]{2,1,0:T(8,128)(2,1)S(1)}, bf16[4,96,256]{2,1,0:T(8,128)(2,1)}, u32[]{:S(2)}) copy-start(bf16[4,96,256]{2,1,0:T(8,128)(2,1)} %get-tuple-element.2) | copy-start | bytes 589828
  (5 other events, 3.5 us)

commit v2 on v1

--- a/solution.py
+++ b/solution.py
@@ -22,6 +22,20 @@
 
 def dot(a, b, da, db):
     return lax.dot_general(a, b, (((da,), (db,)), ((), ())), preferred_element_type=f32)
+
+
+def from_others(array, axis):
+    n = lax.axis_size(axis)
+    later = [
+        lax.ppermute(array, axis, [(i, (i - k) % n) for i in range(n)]) for k in range(1, n)
+    ]
+    return [array, *later]
+
+
+def rolled(array, shift):
+    return lax.dynamic_slice_in_dim(
+        jnp.concatenate([array, array], axis=0), shift, array.shape[0], axis=0
+    )
 
 
 def padded(array, rows):
@@ -41,9 +55,8 @@
         gate_part.reshape(tp, unit, n),
         up_part.reshape(tp, unit, n),
         jnp.broadcast_to(squares.astype(bf16), (tp, 8, n)),
+        *extra,
     ]
-    if extra is not None:
-        tiles.append(extra)
     arrived = exchanged(jnp.concatenate(tiles, axis=1), TP)
     summed = arrived[:, : 2 * unit + 8].astype(f32).sum(axis=0)
     inverse = lax.rsqrt(summed[2 * unit] / D + EPSILON)[None, :]
@@ -81,18 +94,16 @@
     block = width * tp // nz
     piece = block // tp
     halves = width // block
-
-    first = jnp.concatenate([padded(gate_pre.T, unit), padded(up_pre.T, unit)], axis=0)
-    first = gathered(first, "y")
-    gate_pre_t = first[:, :unit].reshape(ny * unit, width)
-    up_pre_t = first[:, unit:].reshape(ny * unit, width)
-
-    down_t = down_pre.T.reshape(halves, tp, piece, units).swapaxes(0, 1)
-    down_t = exchanged(down_t.reshape(tp, halves * piece, units), TP).reshape(width, units)
     kept = query_weight.shape[0]
+
+    all_rows = gathered(residual_in, "z")
+    first = jnp.concatenate(
+        [padded(gate_pre.T, unit), padded(up_pre.T, unit), padded(down_pre, unit)], axis=0
+    )
+    first = from_others(first, "y")
+    first = jnp.stack(first)
     second = jnp.concatenate(
         [
-            padded(down_t.T, unit),
             padded(gate_post.T, unit),
             padded(up_post.T, unit),
             padded(down_post, unit),
@@ -103,54 +114,87 @@
         ],
         axis=0,
     )
-    second = gathered(second, "y")
-    down_pre_all, gate_post_t, up_post_t, down_post_all = (
-        second[:, k * unit : (k + 1) * unit].reshape(ny * unit, width) for k in range(4)
-    )
-    mixers = [
-        second[:, 4 * unit + k * kept : 4 * unit + (k + 1) * kept].reshape(ny * kept, width)
-        for k in range(4)
-    ]
-
-    all_rows = gathered(residual_in, "z").reshape(rows, width)
+    gain_block = lax.dynamic_slice_in_dim(gain_mix, z_at * block, block)
+    gain_block = rolled(gain_block, kept * lax.axis_index("y"))
+    small = jnp.stack([gain_post, head_gain, lower_bound])
+    down_tiles = first[:, 2 * unit :].swapaxes(1, 2).reshape(ny, halves, tp, piece, unit)
+    down_tiles = down_tiles.transpose(2, 0, 1, 3, 4).reshape(tp, ny * halves * piece, unit)
+    all_rows, first, second, gain_block, small, down_tiles = lax.optimization_barrier(
+        (all_rows, first, second, gain_block, small, down_tiles)
+    )
+    gate_pre_t = first[:, :unit].reshape(ny * unit, width)
+    up_pre_t = first[:, unit : 2 * unit].reshape(ny * unit, width)
+
+    all_rows = all_rows.reshape(rows, width)
     turned = all_rows.T.reshape(halves, tp, piece, rows).swapaxes(0, 1)
-    hidden, residual = hidden_units(
-        all_rows, gain_pre, gate_pre_t, up_pre_t, turned.reshape(tp, halves * piece, rows)
+    hidden, extra = hidden_units(
+        all_rows,
+        gain_pre,
+        gate_pre_t,
+        up_pre_t,
+        (turned.reshape(tp, halves * piece, rows), down_tiles),
     )
     residual = lax.dynamic_index_in_dim(
-        residual.reshape(nz, piece, rows), z_at, axis=0, keepdims=False
-    )
-    part = dot(down_pre_all, hidden, 0, 0).astype(bf16)
-    branch = exchanged(part.reshape(nz, piece, rows), "z").astype(f32).sum(axis=0)
+        extra[:, : halves * piece].reshape(nz, piece, rows), z_at, axis=0, keepdims=False
+    )
+    down_pre_t = extra[:, halves * piece :].reshape(tp, ny, halves * piece, unit)
+    part = sum(
+        dot(
+            down_pre_t[:, k].reshape(width, unit),
+            hidden[k * unit : (k + 1) * unit],
+            1,
+            0,
+        )
+        for k in range(ny)
+    ).astype(bf16)
+    second = jnp.stack(from_others(second, "y"))
+    branch = exchanged(part.reshape(nz, piece, rows), "z")
+    branch = branch.astype(f32).sum(axis=0)
     stream_piece = (residual.astype(f32) + 0.5 * branch).astype(bf16)
 
+    gate_post_t, up_post_t, down_post_all = (
+        second[:, k * unit : (k + 1) * unit].reshape(ny * unit, width) for k in range(3)
+    )
+    mixers = jnp.concatenate(
+        [
+            second[:, 3 * unit + k * kept : 3 * unit + (k + 1) * kept].reshape(ny * kept, width)
+            for k in range(4)
+        ],
+        axis=1,
+    )
+    stream_piece, gate_post_t, up_post_t, down_post_all, mixers = lax.optimization_barrier(
+        (stream_piece, gate_post_t, up_post_t, down_post_all, mixers)
+    )
     stream_t = gathered(stream_piece, TP).reshape(block, rows)
     widened = stream_t.astype(f32)
     squares = jnp.sum(widened * widened, axis=0)
-    gain_block = lax.dynamic_slice_in_dim(gain_mix, z_at * block, block)
-    scaled = (widened * gain_block[:, None]).astype(bf16)
-    parts = [dot(scaled, weight, 0, 0).astype(bf16).reshape(nz, own, width) for weight in mixers]
+    scaled = rolled(widened, kept * lax.axis_index("y"))
+    scaled = (scaled * gain_block[:, None]).astype(bf16)
+    heads = width // HEAD_DIM
+    parts = dot(scaled, mixers, 0, 0).astype(bf16)
+    parts = parts.reshape(nz, own, 4 * heads, HEAD_DIM).swapaxes(1, 2)
     mine = z_at // halves == t_at
     note = jnp.where(
         mine,
         stream_t.T.reshape(nz, own, block),
         jnp.broadcast_to(squares.astype(bf16).reshape(nz, own, 1), (nz, own, block)),
     )
-    arrived = exchanged(jnp.concatenate([*parts, note], axis=2), "z")
-    projected = arrived[:, :, : 4 * width].astype(f32).sum(axis=0)
-    notes = arrived[:, :, 4 * width :]
+    message = jnp.concatenate([parts.reshape(nz, 4 * heads * own, HEAD_DIM), note], axis=1)
+    arrived = exchanged(message, "z")
+    projected = arrived[:, : 4 * heads * own].astype(f32).sum(axis=0)
+    notes = arrived[:, 4 * heads * own :]
     stream_a = lax.dynamic_slice_in_dim(notes, t_at * halves, halves, axis=0)
     stream_a = stream_a.swapaxes(0, 1).reshape(own, width).astype(f32)
     elsewhere = (jnp.arange(nz) // halves != t_at)[:, None]
     total = jnp.sum(jnp.where(elsewhere, notes[:, :, 0].astype(f32), 0.0), axis=0)
     total = total + jnp.sum(stream_a * stream_a, axis=1)
+    projected = projected.reshape(4, heads, own, HEAD_DIM)
     projected = projected * lax.rsqrt(total / D + EPSILON)[:, None]
 
-    heads = width // HEAD_DIM
     query_pre, forget_pre, value_pre, outgate_pre = (
-        projected[:, k * width : (k + 1) * width].reshape(own, heads, HEAD_DIM) for k in range(4)
-    )
-    floor_rate = lower_bound.reshape(heads, HEAD_DIM)
+        projected[k].swapaxes(0, 1) for k in range(4)
+    )
+    floor_rate = small[2].reshape(heads, HEAD_DIM)
     log_keep = jnp.logaddexp(
         jnp.log(floor_rate), jnp.log1p(-floor_rate) + jax.nn.log_sigmoid(forget_pre)
     )
@@ -164,7 +208,7 @@
     normed = (
         readout
         * lax.rsqrt(jnp.mean(readout * readout, axis=2, keepdims=True) + EPSILON)
-        * head_gain.reshape(heads, HEAD_DIM)
+        * small[1].reshape(heads, HEAD_DIM)
     )
     mixed_heads = (normed * jax.nn.silu(outgate_pre)).reshape(own, width).astype(bf16)
     partial_out = dot(mixed_heads, out_weight, 1, 0).astype(bf16)
@@ -172,7 +216,7 @@
     stream_b = (stream_a + mixed.astype(f32).sum(axis=0)).astype(bf16)
 
     all_rows = gathered(stream_b, "z").reshape(rows, width)
-    hidden, _ = hidden_units(all_rows, gain_post, gate_post_t, up_post_t, None)
+    hidden, _ = hidden_units(all_rows, small[0], gate_post_t, up_post_t, ())
     part = dot(hidden, down_post_all, 0, 0).astype(bf16)
     branch = exchanged(part.reshape(nz, own, width), "z").astype(f32).sum(axis=0)
     layer_out = (stream_b.astype(f32) + 0.5 * branch).astype(bf16)
@@ -203,4 +247,5 @@
         P(kv, TP, None, None),
     )
     out_specs = (P(kv, TP), P(kv, TP, None, None))
+
     return jax.shard_map(shards, mesh=grid, in_specs=in_specs, out_specs=out_specs, check_vma=False)

time: 213 us -> 203 us (0.953)
  waiting for transfers between devices: 68.8 us -> 46.3 us
  starting transfers between devices: 53.1 us -> 63.4 us
    all_to_all x9 -> x6, waiting for transfers between devices: 68.8 us -> 46.3 us  [exchanged(): return lax.all_to_all(tiles, axis, split_axis=0, concat_axis=0, tiled=True)]
    ppermute x0 -> x6, starting transfers between devices: none -> 20 us  [from_others(): lax.ppermute(array, axis, [(i, (i - k) % n) for i in range(n)])]
    all_to_all x9 -> x6, starting transfers between devices: 53.1 us -> 43.4 us  [exchanged(): return lax.all_to_all(tiles, axis, split_axis=0, concat_axis=0, tiled=True)]
    unnamed x54 -> x56, local copies, waits for them, and re-layouts: 9.13 us -> 12.7 us
    broadcast_in_dim x7 -> x5, local copies, waits for them, and re-layouts: 4.53 us -> 1.99 us  [gathered(): jnp.broadcast_to(array, (lax.axis_size(axis), *array.shape))]
  transfers between devices with their start and end apart: 9 -> 12, of which waited for: 9 -> 6; matrix products, arithmetic and copies ran while one was open for 3% -> 4% of each run, Pallas kernels for 0% -> 0%
where the time goes in v2:
time: 203 us; the launch traced here: 201 us
  starting transfers between devices  63.4 us (31%)
  blocking collectives  61.6 us (30%)
  waiting for transfers between devices  46.3 us (23%)
  local copies, waits for them, and re-layouts  20.5 us (10%)
  other arithmetic  4.69 us (2%)
  matrix products  3.24 us (2%)
    all_to_all x5, blocking collectives, exchanged(): return lax.all_to_all(tiles, axis, split_axis=0, concat_axis=0, tiled=True)  61.6 us
    all_to_all x6, waiting for transfers between devices, exchanged(): return lax.all_to_all(tiles, axis, split_axis=0, concat_axis=0, tiled=True)  46.3 us
    all_to_all x6, starting transfers between devices, exchanged(): return lax.all_to_all(tiles, axis, split_axis=0, concat_axis=0, tiled=True)  43.4 us
    ppermute x6, starting transfers between devices, from_others(): lax.ppermute(array, axis, [(i, (i - k) % n) for i in range(n)])  20 us
    unnamed x56, local copies, waits for them, and re-layouts  12.7 us
  transfers between devices with their start and end apart: 12, of which 6 were waited for; matrix products, arithmetic and copies ran while one was open for 4% of the time, Pallas kernels for 0%

profile of v2, /device:TPU:1, one launch (start us, length us, event | category | flops | bytes accessed | tf_op | source)
XLA Modules:
  0.0 201.0 jit_solution(6928826120703163837)
XLA Ops:
  2.7 4.0 %collective-permute-start.2 = (bf16[288,256]{0,1:T(8,128)(2,1)S(1)}, bf16[288,256]{0,1:T(8,128)(2,1)S(1)}, u32[]{:S(2)}, u32[]{:S(2)}) collective-permute-start(bf16[288,256]{0,1:T(8,128)(2,1)S(1)} %fusion.7), channel_id=1, source_target_pairs={{0,8},{8,16},{16,24},{24,0},{1,9},{9,17},{17,25},{25,1},{2,10},{10... | collective-permute-start | bytes 442376 | tf_op jit(solution)/shard_map/ppermute | solution.py:30
  6.8 4.5 %collective-permute-start.1 = (bf16[288,256]{0,1:T(8,128)(2,1)S(1)}, bf16[288,256]{0,1:T(8,128)(2,1)S(1)}, u32[]{:S(2)}, u32[]{:S(2)}) collective-permute-start(bf16[288,256]{0,1:T(8,128)(2,1)S(1)} %fusion.7), channel_id=1, source_target_pairs={{0,16},{8,24},{16,0},{24,8},{1,17},{9,25},{17,1},{25,9},{2,18},{10... | collective-permute-start | bytes 442376 | tf_op jit(solution)/shard_map/ppermute | solution.py:30
  11.3 3.0 %collective-permute-start = (bf16[288,256]{0,1:T(8,128)(2,1)S(1)}, bf16[288,256]{0,1:T(8,128)(2,1)S(1)}, u32[]{:S(2)}, u32[]{:S(2)}) collective-permute-start(bf16[288,256]{0,1:T(8,128)(2,1)S(1)} %fusion.7), channel_id=1, source_target_pairs={{0,24},{8,0},{16,8},{24,16},{1,25},{9,1},{17,9},{25,17},{2,26},{10... | collective-permute-start | bytes 442376 | tf_op jit(solution)/shard_map/ppermute | solution.py:30
  14.9 14.9 %all-to-all-start = ((bf16[16,6,256]{2,1,0:T(8,128)(2,1)}), bf16[16,6,256]{2,1,0:T(8,128)(2,1)S(1)}, u32[]{:S(2)}, u32[]{:S(2)}) async-start(bf16[16,6,256]{2,1,0:T(8,128)(2,1)} %broadcast_in_dim.28), calls=%async_computation | async-start | bytes 131072 | tf_op jit(solution)/shard_map/all_to_all | solution.py:16
  38.2 3.2 %all-to-all-done = bf16[16,6,256]{2,1,0:T(8,128)(2,1)S(1)} async-done(((bf16[16,6,256]{2,1,0:T(8,128)(2,1)}), bf16[16,6,256]{2,1,0:T(8,128)(2,1)S(1)}, u32[]{:S(2)}, u32[]{:S(2)}) %all-to-all-start) | async-done | bytes 49184 | tf_op jit(solution)/shard_map/all_to_all | solution.py:16
  41.4 2.3 %collective-permute-start.5 = (bf16[416,256]{1,0:T(8,128)(2,1)S(1)}, bf16[416,256]{1,0:T(8,128)(2,1)S(1)}, u32[]{:S(2)}, u32[]{:S(2)}) collective-permute-start(bf16[416,256]{1,0:T(8,128)(2,1)S(1)} %constant_dynamic-update-slice_fusion), channel_id=1, source_target_pairs={{0,8},{8,16},{16,24},{24,0},{1,9},{9,17},{17,25},{25,1},{2,10},{10... | collective-permute-start | bytes 638984 | tf_op jit(solution)/shard_map/ppermute | solution.py:30
  43.7 2.8 %collective-permute-start.4 = (bf16[416,256]{1,0:T(8,128)(2,1)S(1)}, bf16[416,256]{1,0:T(8,128)(2,1)S(1)}, u32[]{:S(2)}, u32[]{:S(2)}) collective-permute-start(bf16[416,256]{1,0:T(8,128)(2,1)S(1)} %constant_dynamic-update-slice_fusion), channel_id=1, source_target_pairs={{0,16},{8,24},{16,0},{24,8},{1,17},{9,25},{17,1},{25,9},{2,18},{10... | collective-permute-start | bytes 638984 | tf_op jit(solution)/shard_map/ppermute | solution.py:30
  46.5 3.4 %collective-permute-start.3 = (bf16[416,256]{1,0:T(8,128)(2,1)S(1)}, bf16[416,256]{1,0:T(8,128)(2,1)S(1)}, u32[]{:S(2)}, u32[]{:S(2)}) collective-permute-start(bf16[416,256]{1,0:T(8,128)(2,1)S(1)} %constant_dynamic-update-slice_fusion), channel_id=1, source_target_pairs={{0,24},{8,0},{16,8},{24,16},{1,25},{9,1},{17,9},{25,17},{2,26},{10... | collective-permute-start | bytes 638984 | tf_op jit(solution)/shard_map/ppermute | solution.py:30
  55.4 7.9 %all-to-all-start.1 = ((bf16[8,264,96]{2,1,0:T(8,128)(2,1)}), bf16[8,264,96]{2,1,0:T(8,128)(2,1)S(1)}, u32[]{:S(2)}, u32[]{:S(2)}) async-start(bf16[8,264,96]{2,1,0:T(8,128)(2,1)} %constant_dynamic-update-slice_fusion.4), calls=%async_computation.1 | async-start | bytes 1081344 | tf_op jit(solution)/shard_map/all_to_all | solution.py:16
  63.6 9.3 %all-to-all-done.1 = bf16[8,264,96]{2,1,0:T(8,128)(2,1)S(1)} async-done(((bf16[8,264,96]{2,1,0:T(8,128)(2,1)}), bf16[8,264,96]{2,1,0:T(8,128)(2,1)S(1)}, u32[]{:S(2)}, u32[]{:S(2)}) %all-to-all-start.1) | async-done | bytes 405536 | tf_op jit(solution)/shard_map/all_to_all | solution.py:16
  73.7 4.2 %all-to-all-start.2 = ((bf16[8,48,96]{2,1,0:T(8,128)(2,1)}), bf16[8,48,96]{2,1,0:T(8,128)(2,1)S(1)}, u32[]{:S(2)}, u32[]{:S(2)}) async-start(bf16[8,48,96]{2,1,0:T(8,128)(2,1)} %broadcast_in_dim.52), calls=%async_computation.2 | async-start | bytes 196608 | tf_op jit(solution)/shard_map/all_to_all | solution.py:16
  78.0 5.0 %all-to-all-done.2 = bf16[8,48,96]{2,1,0:T(8,128)(2,1)S(1)} async-done(((bf16[8,48,96]{2,1,0:T(8,128)(2,1)}), bf16[8,48,96]{2,1,0:T(8,128)(2,1)S(1)}, u32[]{:S(2)}, u32[]{:S(2)}) %all-to-all-start.2) | async-done | bytes 73760 | tf_op jit(solution)/shard_map/all_to_all | solution.py:16
  84.6 7.3 %all-to-all-start.3 = ((bf16[16,16,96]{2,1,0:T(8,128)(2,1)}), bf16[16,16,96]{2,1,0:T(8,128)(2,1)S(1)}, u32[]{:S(2)}, u32[]{:S(2)}) async-start(bf16[16,16,96]{2,1,0:T(8,128)(2,1)} %bitcast.35), calls=%async_computation.3 | async-start | bytes 131072 | tf_op jit(solution)/shard_map/all_to_all | solution.py:16
  91.9 11.5 %all-to-all-done.3 = bf16[16,16,96]{2,1,0:T(8,128)(2,1)S(1)} async-done(((bf16[16,16,96]{2,1,0:T(8,128)(2,1)}), bf16[16,16,96]{2,1,0:T(8,128)(2,1)S(1)}, u32[]{:S(2)}, u32[]{:S(2)}) %all-to-all-start.3) | async-done | bytes 49184 | tf_op jit(solution)/shard_map/all_to_all | solution.py:16
  104.1 5.5 %all-to-all-start.4 = ((bf16[8,16,96]{2,1,0:T(8,128)(2,1)}), bf16[8,16,96]{2,1,0:T(8,128)(2,1)S(1)}, u32[]{:S(2)}, u32[]{:S(2)}) async-start(bf16[8,16,96]{2,1,0:T(8,128)(2,1)} %broadcast_in_dim.53), calls=%async_computation.4 | async-start | bytes 65536 | tf_op jit(solution)/shard_map/all_to_all | solution.py:16
  109.6 4.7 %all-to-all-done.4 = bf16[8,16,96]{2,1,0:T(8,128)(2,1)S(1)} async-done(((bf16[8,16,96]{2,1,0:T(8,128)(2,1)}), bf16[8,16,96]{2,1,0:T(8,128)(2,1)S(1)}, u32[]{:S(2)}, u32[]{:S(2)}) %all-to-all-start.4) | async-done | bytes 24608 | tf_op jit(solution)/shard_map/all_to_all | solution.py:16
  116.7 3.5 %all-to-all-start.5 = ((bf16[16,54,128]{2,1,0:T(8,128)(2,1)}), bf16[16,54,128]{2,1,0:T(8,128)(2,1)S(1)}, u32[]{:S(2)}, u32[]{:S(2)}) async-start(bf16[16,54,128]{2,1,0:T(8,128)(2,1)} %copy.153), calls=%async_computation.5 | async-start | bytes 458752 | tf_op jit(solution)/shard_map/all_to_all | solution.py:16
  120.9 12.6 %all-to-all-done.5 = bf16[16,54,128]{2,1,0:T(8,128)(2,1)S(1)} async-done(((bf16[16,54,128]{2,1,0:T(8,128)(2,1)}), bf16[16,54,128]{2,1,0:T(8,128)(2,1)S(1)}, u32[]{:S(2)}, u32[]{:S(2)}) %all-to-all-start.5) | async-done | bytes 221216 | tf_op jit(solution)/shard_map/all_to_all | solution.py:16
  134.1 1.6 multiply_add_fusion
  136.9 11.6 %all_to_all.55 = bf16[8,6,256]{2,1,0:T(8,128)(2,1)S(1)} all-to-all(bf16[8,6,256]{2,1,0:T(8,128)(2,1)S(1)} %bitcast.214), channel_id=1, replica_groups=mesh['z'=16,'y'=4,'x'=4,'c'=2] {'x','c'}, dimensions={0} | all-to-all | bytes 49152 | tf_op jit(solution)/shard_map/all_to_all | solution.py:16
  148.5 17.0 %all_to_all.56 = bf16[16,6,256]{2,1,0:T(8,128)(2,1)S(1)} all-to-all(bf16[16,6,256]{2,1,0:T(8,128)(2,1)S(1)} %broadcast_in_dim.57), channel_id=1, replica_groups=mesh['z'=16,'y'=4,'x'=4,'c'=2] {'z'}, dimensions={0} | all-to-all | bytes 98304 | tf_op jit(solution)/shard_map/all_to_all | solution.py:16
  166.6 10.4 %all_to_all.57 = bf16[8,104,96]{1,2,0:T(8,128)(2,1)S(1)} all-to-all(bf16[8,104,96]{1,2,0:T(8,128)(2,1)S(1)} %copy.161), channel_id=1, replica_groups=mesh['z'=16,'y'=4,'x'=4,'c'=2] {'x','c'}, dimensions={0} | all-to-all | bytes 319488 | tf_op jit(solution)/shard_map/all_to_all | solution.py:16
  177.6 8.3 %all_to_all.58 = bf16[8,48,96]{2,1,0:T(8,128)(2,1)S(1)} all-to-all(bf16[8,48,96]{2,1,0:T(8,128)(2,1)S(1)} %broadcast_in_dim.59), channel_id=1, replica_groups=mesh['z'=16,'y'=4,'x'=4,'c'=2] {'x','c'}, dimensions={0} | all-to-all | bytes 147456 | tf_op jit(solution)/shard_map/all_to_all | solution.py:16
  186.1 14.3 %all_to_all.59 = bf16[16,6,256]{2,1,0:T(8,128)(2,1)S(1)} all-to-all(bf16[16,6,256]{2,1,0:T(8,128)(2,1)S(1)} %reshape.221), channel_id=1, replica_groups=mesh['z'=16,'y'=4,'x'=4,'c'=2] {'z'}, dimensions={0} | all-to-all | bytes 98304 | tf_op jit(solution)/shard_map/all_to_all | solution.py:16
  (160 shorter events, 26.8 us)
Async XLA Ops:
  0.6 136.0 %copy-start = (bf16[256,2048]{1,0:T(8,128)(2,1)S(1)}, bf16[256,2048]{1,0:T(8,128)(2,1)}, u32[]{:S(2)}) copy-start(bf16[256,2048]{1,0:T(8,128)(2,1)} %param.30) | copy-start | bytes 3145732
  0.6 1.0 copy-start.3
  1.7 0.8 copy-start.4
  2.6 11.7 %copy-start.13 = (bf16[6,256]{1,0:T(8,128)(2,1)S(1)}, bf16[6,256]{1,0:T(8,128)(2,1)}, u32[]{:S(2)}) copy-start(bf16[6,256]{1,0:T(8,128)(2,1)} %param.18) | copy-start | bytes 9220
  2.7 35.1 %collective-permute-start.2 = (bf16[288,256]{0,1:T(8,128)(2,1)S(1)}, bf16[288,256]{0,1:T(8,128)(2,1)S(1)}, u32[]{:S(2)}, u32[]{:S(2)}) collective-permute-start(bf16[288,256]{0,1:T(8,128)(2,1)S(1)} %fusion.7), channel_id=1, source_target_pairs={{0,8},{8,16},{16,24},{24,0},{1,9},{9,17},{17,25},{25,1},{2,10},{10... | collective-permute-start | bytes 442376 | tf_op jit(solution)/shard_map/ppermute | solution.py:30
  6.8 31.1 %collective-permute-start.1 = (bf16[288,256]{0,1:T(8,128)(2,1)S(1)}, bf16[288,256]{0,1:T(8,128)(2,1)S(1)}, u32[]{:S(2)}, u32[]{:S(2)}) collective-permute-start(bf16[288,256]{0,1:T(8,128)(2,1)S(1)} %fusion.7), channel_id=1, source_target_pairs={{0,16},{8,24},{16,0},{24,8},{1,17},{9,25},{17,1},{25,9},{2,18},{10... | collective-permute-start | bytes 442376 | tf_op jit(solution)/shard_map/ppermute | solution.py:30
  11.3 26.5 %collective-permute-start = (bf16[288,256]{0,1:T(8,128)(2,1)S(1)}, bf16[288,256]{0,1:T(8,128)(2,1)S(1)}, u32[]{:S(2)}, u32[]{:S(2)}) collective-permute-start(bf16[288,256]{0,1:T(8,128)(2,1)S(1)} %fusion.7), channel_id=1, source_target_pairs={{0,24},{8,0},{16,8},{24,16},{1,25},{9,1},{17,9},{25,17},{2,26},{10... | collective-permute-start | bytes 442376 | tf_op jit(solution)/shard_map/ppermute | solution.py:30
  14.9 26.5 %all-to-all-start = ((bf16[16,6,256]{2,1,0:T(8,128)(2,1)}), bf16[16,6,256]{2,1,0:T(8,128)(2,1)S(1)}, u32[]{:S(2)}, u32[]{:S(2)}) async-start(bf16[16,6,256]{2,1,0:T(8,128)(2,1)} %broadcast_in_dim.28), calls=%async_computation | async-start | bytes 131072 | tf_op jit(solution)/shard_map/all_to_all | solution.py:16
  29.9 0.8 copy-start.5
  30.6 0.8 copy-start.6
  31.4 0.8 copy-start.7
  32.2 0.7 copy-start.8
  32.9 0.7 copy-start.9
  41.4 22.0 %collective-permute-start.5 = (bf16[416,256]{1,0:T(8,128)(2,1)S(1)}, bf16[416,256]{1,0:T(8,128)(2,1)S(1)}, u32[]{:S(2)}, u32[]{:S(2)}) collective-permute-start(bf16[416,256]{1,0:T(8,128)(2,1)S(1)} %constant_dynamic-update-slice_fusion), channel_id=1, source_target_pairs={{0,8},{8,16},{16,24},{24,0},{1,9},{9,17},{17,25},{25,1},{2,10},{10... | collective-permute-start | bytes 638984 | tf_op jit(solution)/shard_map/ppermute | solution.py:30
  43.7 19.7 %collective-permute-start.4 = (bf16[416,256]{1,0:T(8,128)(2,1)S(1)}, bf16[416,256]{1,0:T(8,128)(2,1)S(1)}, u32[]{:S(2)}, u32[]{:S(2)}) collective-permute-start(bf16[416,256]{1,0:T(8,128)(2,1)S(1)} %constant_dynamic-update-slice_fusion), channel_id=1, source_target_pairs={{0,16},{8,24},{16,0},{24,8},{1,17},{9,25},{17,1},{25,9},{2,18},{10... | collective-permute-start | bytes 638984 | tf_op jit(solution)/shard_map/ppermute | solution.py:30
  46.5 16.8 %collective-permute-start.3 = (bf16[416,256]{1,0:T(8,128)(2,1)S(1)}, bf16[416,256]{1,0:T(8,128)(2,1)S(1)}, u32[]{:S(2)}, u32[]{:S(2)}) collective-permute-start(bf16[416,256]{1,0:T(8,128)(2,1)S(1)} %constant_dynamic-update-slice_fusion), channel_id=1, source_target_pairs={{0,24},{8,0},{16,8},{24,16},{1,25},{9,1},{17,9},{25,17},{2,26},{10... | collective-permute-start | bytes 638984 | tf_op jit(solution)/shard_map/ppermute | solution.py:30
  55.4 17.5 %all-to-all-start.1 = ((bf16[8,264,96]{2,1,0:T(8,128)(2,1)}), bf16[8,264,96]{2,1,0:T(8,128)(2,1)S(1)}, u32[]{:S(2)}, u32[]{:S(2)}) async-start(bf16[8,264,96]{2,1,0:T(8,128)(2,1)} %constant_dynamic-update-slice_fusion.4), calls=%async_computation.1 | async-start | bytes 1081344 | tf_op jit(solution)/shard_map/all_to_all | solution.py:16
  72.9 19.0 %copy-start.2 = (bf16[8,264,96]{2,1,0:T(8,128)(2,1)}, bf16[8,264,96]{2,1,0:T(8,128)(2,1)S(1)}, u32[]{:S(2)}) copy-start(bf16[8,264,96]{2,1,0:T(8,128)(2,1)S(1)} %all-to-all-done.1) | copy-start | bytes 1216516
  73.7 9.2 %all-to-all-start.2 = ((bf16[8,48,96]{2,1,0:T(8,128)(2,1)}), bf16[8,48,96]{2,1,0:T(8,128)(2,1)S(1)}, u32[]{:S(2)}, u32[]{:S(2)}) async-start(bf16[8,48,96]{2,1,0:T(8,128)(2,1)} %broadcast_in_dim.52), calls=%async_computation.2 | async-start | bytes 196608 | tf_op jit(solution)/shard_map/all_to_all | solution.py:16
  84.6 18.9 %all-to-all-start.3 = ((bf16[16,16,96]{2,1,0:T(8,128)(2,1)}), bf16[16,16,96]{2,1,0:T(8,128)(2,1)S(1)}, u32[]{:S(2)}, u32[]{:S(2)}) async-start(bf16[16,16,96]{2,1,0:T(8,128)(2,1)} %bitcast.35), calls=%async_computation.3 | async-start | bytes 131072 | tf_op jit(solution)/shard_map/all_to_all | solution.py:16
  91.9 11.6 %slice-start = ((bf16[8,264,96]{2,1,0:T(8,128)(2,1)}), bf16[8,32,96]{2,1,0:T(8,128)(2,1)S(1)}, s32[]{:S(2)}) async-start(bf16[8,264,96]{2,1,0:T(8,128)(2,1)} %copy-done.2), calls=%async_computation.11 | async-start | bytes 131072 | tf_op jit(solution)/shard_map/slice | solution.py:138
  104.1 10.2 %all-to-all-start.4 = ((bf16[8,16,96]{2,1,0:T(8,128)(2,1)}), bf16[8,16,96]{2,1,0:T(8,128)(2,1)S(1)}, u32[]{:S(2)}, u32[]{:S(2)}) async-start(bf16[8,16,96]{2,1,0:T(8,128)(2,1)} %broadcast_in_dim.53), calls=%async_computation.4 | async-start | bytes 65536 | tf_op jit(solution)/shard_map/all_to_all | solution.py:16
  116.7 16.8 %all-to-all-start.5 = ((bf16[16,54,128]{2,1,0:T(8,128)(2,1)}), bf16[16,54,128]{2,1,0:T(8,128)(2,1)S(1)}, u32[]{:S(2)}, u32[]{:S(2)}) async-start(bf16[16,54,128]{2,1,0:T(8,128)(2,1)} %copy.153), calls=%async_computation.5 | async-start | bytes 458752 | tf_op jit(solution)/shard_map/all_to_all | solution.py:16
  135.7 1.2 copy-start.1
  (8 other events, 5.6 us)

commit v3 on v2

--- a/solution.py
+++ b/solution.py
@@ -1,6 +1,8 @@
 import jax
 import jax.numpy as jnp
 from jax import lax
+from jax.experimental import pallas as pl
+from jax.experimental.pallas import tpu as pltpu
 from jax.sharding import Mesh, PartitionSpec as P
 
 D = 2048
@@ -32,14 +34,65 @@
     return [array, *later]
 
 
-def rolled(array, shift):
-    return lax.dynamic_slice_in_dim(
-        jnp.concatenate([array, array], axis=0), shift, array.shape[0], axis=0
-    )
-
-
-def padded(array, rows):
-    return jnp.pad(array, ((0, rows - array.shape[0]), (0, 0)))
+def staged(unit, copies, ups, downs, kept, small):
+    rows, gate_a, up_a, down_a, gate_b, up_b, down_b, *projections = ups + downs + kept
+    units, width = gate_a.shape
+    height = projections[0].shape[0]
+    n_in = 7 + len(projections) + len(small)
+
+    def kernel(*refs):
+        ins, outs = refs[:n_in], refs[n_in : n_in + 3 + len(small)]
+        held, sems = refs[-2], refs[-1]
+        spread, first, second = outs[:3]
+        moves = [(ins[0], held)]
+        moves += [(ins[1 + k], first.at[pl.ds(k * unit, units)]) for k in range(3)]
+        moves += [(ins[4 + k], second.at[pl.ds(k * unit, units)]) for k in range(3)]
+        for k in range(len(projections)):
+            moves.append((ins[7 + k], second.at[pl.ds(3 * unit + k * height, height)]))
+        for k in range(len(small)):
+            moves.append((ins[7 + len(projections) + k], outs[3 + k]))
+        started = [pltpu.make_async_copy(a, b, sems.at[k]) for k, (a, b) in enumerate(moves)]
+        for move in started:
+            move.start()
+        if unit > units:
+            blank = jnp.zeros((unit - units, width), first.dtype)
+            for k in range(3):
+                first[pl.ds(k * unit + units, unit - units), :] = blank
+                second[pl.ds(k * unit + units, unit - units), :] = blank
+        started[0].wait()
+        for k in range(copies):
+            spread[k] = held[...]
+        for move in started[1:]:
+            move.wait()
+
+    arrays = [rows, gate_a, up_a, down_a, gate_b, up_b, down_b, *projections, *small]
+    vmem = pl.BlockSpec(memory_space=pltpu.VMEM)
+    shapes = [
+        jax.ShapeDtypeStruct((copies, *rows.shape), bf16),
+        jax.ShapeDtypeStruct((3 * unit, width), bf16),
+        jax.ShapeDtypeStruct((3 * unit + len(projections) * height, width), bf16),
+        *[jax.ShapeDtypeStruct(v.shape, v.dtype) for v in small],
+    ]
+    return pl.pallas_call(
+        kernel,
+        out_shape=shapes,
+        in_specs=[pl.BlockSpec(memory_space=pl.ANY)] * n_in,
+        out_specs=[vmem] * len(shapes),
+        scratch_shapes=[pltpu.VMEM(rows.shape, bf16), pltpu.SemaphoreType.DMA((n_in,))],
+    )(*arrays)
+
+
+def doubled(array, axis, apart):
+    n = lax.axis_size(axis)
+    return jnp.concatenate([array, lax.ppermute(array, axis, [(i, i ^ apart) for i in range(n)])])
+
+
+def reordered(blocks, at):
+    blocks = jnp.stack([blocks[0], blocks[2], blocks[1], blocks[3]])
+    halves = jnp.concatenate([blocks[2:], blocks[:2]])
+    blocks = jnp.where(at % 2 == 1, halves, blocks)
+    pairs = jnp.concatenate([blocks[1:2], blocks[0:1], blocks[3:4], blocks[2:3]])
+    return jnp.where(at // 2 == 1, pairs, blocks)
 
 
 def hidden_units(rows, gain_vec, gate_t, up_t, extra):
@@ -96,31 +149,25 @@
     halves = width // block
     kept = query_weight.shape[0]
 
-    all_rows = gathered(residual_in, "z")
-    first = jnp.concatenate(
-        [padded(gate_pre.T, unit), padded(up_pre.T, unit), padded(down_pre, unit)], axis=0
-    )
+    y_at = lax.axis_index("y")
+    spread, first, second, gain_pre, gain_post, head_gain, lower_bound, gain_mix = staged(
+        unit,
+        nz,
+        [residual_in, gate_pre.T, up_pre.T],
+        [down_pre, gate_post.T, up_post.T, down_post],
+        [query_weight, forget_weight, value_weight, outgate_weight],
+        [v.reshape(-1, HEAD_DIM) for v in (gain_pre, gain_post, head_gain, lower_bound, gain_mix)],
+    )
+    gain_pre, gain_post = gain_pre.reshape(width), gain_post.reshape(width)
+    gain_block = lax.dynamic_slice_in_dim(gain_mix, z_at * block // HEAD_DIM, block // HEAD_DIM)
+    gain_block = reordered(gain_block.reshape(ny, kept), y_at).reshape(block)
     first = from_others(first, "y")
+    all_rows = exchanged(spread, "z")
     first = jnp.stack(first)
-    second = jnp.concatenate(
-        [
-            padded(gate_post.T, unit),
-            padded(up_post.T, unit),
-            padded(down_post, unit),
-            query_weight,
-            forget_weight,
-            value_weight,
-            outgate_weight,
-        ],
-        axis=0,
-    )
-    gain_block = lax.dynamic_slice_in_dim(gain_mix, z_at * block, block)
-    gain_block = rolled(gain_block, kept * lax.axis_index("y"))
-    small = jnp.stack([gain_post, head_gain, lower_bound])
     down_tiles = first[:, 2 * unit :].swapaxes(1, 2).reshape(ny, halves, tp, piece, unit)
     down_tiles = down_tiles.transpose(2, 0, 1, 3, 4).reshape(tp, ny * halves * piece, unit)
-    all_rows, first, second, gain_block, small, down_tiles = lax.optimization_barrier(
-        (all_rows, first, second, gain_block, small, down_tiles)
+    all_rows, first, gain_block, down_tiles = lax.optimization_barrier(
+        (all_rows, first, gain_block, down_tiles)
     )
     gate_pre_t = first[:, :unit].reshape(ny * unit, width)
     up_pre_t = first[:, unit : 2 * unit].reshape(ny * unit, width)
@@ -147,7 +194,8 @@
         )
         for k in range(ny)
     ).astype(bf16)
-    second = jnp.stack(from_others(second, "y"))
+    second = doubled(second, "y", 2)
+    second = doubled(second, "y", 1).reshape(ny, -1, width)
     branch = exchanged(part.reshape(nz, piece, rows), "z")
     branch = branch.astype(f32).sum(axis=0)
     stream_piece = (residual.astype(f32) + 0.5 * branch).astype(bf16)
@@ -168,7 +216,7 @@
     stream_t = gathered(stream_piece, TP).reshape(block, rows)
     widened = stream_t.astype(f32)
     squares = jnp.sum(widened * widened, axis=0)
-    scaled = rolled(widened, kept * lax.axis_index("y"))
+    scaled = reordered(widened.reshape(ny, kept, rows), y_at).reshape(block, rows)
     scaled = (scaled * gain_block[:, None]).astype(bf16)
     heads = width // HEAD_DIM
     parts = dot(scaled, mixers, 0, 0).astype(bf16)
@@ -194,7 +242,7 @@
     query_pre, forget_pre, value_pre, outgate_pre = (
         projected[k].swapaxes(0, 1) for k in range(4)
     )
-    floor_rate = small[2].reshape(heads, HEAD_DIM)
+    floor_rate = lower_bound.reshape(heads, HEAD_DIM)
     log_keep = jnp.logaddexp(
         jnp.log(floor_rate), jnp.log1p(-floor_rate) + jax.nn.log_sigmoid(forget_pre)
     )
@@ -208,7 +256,7 @@
     normed = (
         readout
         * lax.rsqrt(jnp.mean(readout * readout, axis=2, keepdims=True) + EPSILON)
-        * small[1].reshape(heads, HEAD_DIM)
+        * head_gain.reshape(heads, HEAD_DIM)
     )
     mixed_heads = (normed * jax.nn.silu(outgate_pre)).reshape(own, width).astype(bf16)
     partial_out = dot(mixed_heads, out_weight, 1, 0).astype(bf16)
@@ -216,7 +264,7 @@
     stream_b = (stream_a + mixed.astype(f32).sum(axis=0)).astype(bf16)
 
     all_rows = gathered(stream_b, "z").reshape(rows, width)
-    hidden, _ = hidden_units(all_rows, small[0], gate_post_t, up_post_t, ())
+    hidden, _ = hidden_units(all_rows, gain_post, gate_post_t, up_post_t, ())
     part = dot(hidden, down_post_all, 0, 0).astype(bf16)
     branch = exchanged(part.reshape(nz, own, width), "z").astype(f32).sum(axis=0)
     layer_out = (stream_b.astype(f32) + 0.5 * branch).astype(bf16)

time: 203 us -> 190 us (0.936)
  local copies, waits for them, and re-layouts: 20.5 us -> 9.33 us
  starting transfers between devices: 63.4 us -> 57.6 us
  waiting for transfers between devices: 46.3 us -> 50.3 us
    ppermute x6 -> x3, starting transfers between devices: 20 us -> 10.3 us  [from_others(): lax.ppermute(array, axis, [(i, (i - k) % n) for i in range(n)])]
    unnamed x56 -> x27, local copies, waits for them, and re-layouts: 12.7 us -> 3.02 us
    ppermute x0 -> x2, starting transfers between devices: none -> 7.1 us  [doubled(): lax.ppermute(array, axis, [(i, i ^ apart) for i in range(n)])]
    ppermute x0 -> x2, waiting for transfers between devices: none -> 6.59 us  [doubled(): lax.ppermute(array, axis, [(i, i ^ apart) for i in range(n)])]
    all_to_all x6, starting transfers between devices: 43.4 us -> 40.2 us  [exchanged(): return lax.all_to_all(tiles, axis, split_axis=0, concat_axis=0, tiled=True)]
    all_to_all x6, waiting for transfers between devices: 46.3 us -> 43.7 us  [exchanged(): return lax.all_to_all(tiles, axis, split_axis=0, concat_axis=0, tiled=True)]
  transfers between devices with their start and end apart: 12 -> 11, of which waited for: 6 -> 6; matrix products, arithmetic and copies ran while one was open for 4% -> 2% of each run, Pallas kernels for 0% -> 0%
where the time goes in v3:
time: 190 us; the launch traced here: 189 us
  blocking collectives  61.6 us (32%)
  starting transfers between devices  57.6 us (30%)
  waiting for transfers between devices  50.3 us (26%)
  local copies, waits for them, and re-layouts  9.33 us (5%)
  other arithmetic  3.59 us (2%)
  matrix products  3.12 us (2%)
  Pallas kernels  1.92 us (1%)
    all_to_all x5, blocking collectives, exchanged(): return lax.all_to_all(tiles, axis, split_axis=0, concat_axis=0, tiled=True)  61.6 us
    all_to_all x6, waiting for transfers between devices, exchanged(): return lax.all_to_all(tiles, axis, split_axis=0, concat_axis=0, tiled=True)  43.7 us
    all_to_all x6, starting transfers between devices, exchanged(): return lax.all_to_all(tiles, axis, split_axis=0, concat_axis=0, tiled=True)  40.2 us
    ppermute x3, starting transfers between devices, from_others(): lax.ppermute(array, axis, [(i, (i - k) % n) for i in range(n)])  10.3 us
    ppermute x2, starting transfers between devices, doubled(): lax.ppermute(array, axis, [(i, i ^ apart) for i in range(n)])  7.1 us
    ppermute x2, waiting for transfers between devices, doubled(): lax.ppermute(array, axis, [(i, i ^ apart) for i in range(n)])  6.59 us
  transfers between devices with their start and end apart: 11, of which 6 were waited for; matrix products, arithmetic and copies ran while one was open for 2% of the time, Pallas kernels for 0%

profile of v3, /device:TPU:1, one launch (start us, length us, event | category | flops | bytes accessed | tf_op | source)
XLA Modules:
  0.0 188.9 jit_solution(2229123727231958479)
XLA Ops:
  0.7 1.9 %shard_map.185 = (bf16[16,6,256]{2,1,0:T(8,128)(2,1)}, bf16[288,256]{1,0:T(8,128)(2,1)}, bf16[416,256]{1,0:T(8,128)(2,1)}, f32[2,128]{1,0:T(2,128)}, f32[2,128]{...) custom-call(bf16[6,256]{1,0:T(8,128)(2,1)} %refs_0_.1, bf16[88,256]{1,0:T(8,128)(2,1)} %bitcast.218, ...), custom_call_target="tpu_custom_call" | custom-call | tf_op jit(solution)/shard_map/pallas_call | solution.py:76
  2.6 5.5 %collective-permute-start = (bf16[288,256]{1,0:T(8,128)(2,1)}, bf16[288,256]{1,0:T(8,128)(2,1)S(1)}, u32[]{:S(2)}, u32[]{:S(2)}) collective-permute-start(bf16[288,256]{1,0:T(8,128)(2,1)} %get-tuple-element.20), channel_id=1, source_target_pairs={{0,24},{8,0},{16,8},{24,16},{1,25},{9,1},{17,9},{25,17},{2,26},{10... | collective-permute-start | bytes 442376 | tf_op jit(solution)/shard_map/ppermute | solution.py:32
  8.1 2.3 %collective-permute-start.1 = (bf16[288,256]{1,0:T(8,128)(2,1)}, bf16[288,256]{1,0:T(8,128)(2,1)S(1)}, u32[]{:S(2)}, u32[]{:S(2)}) collective-permute-start(bf16[288,256]{1,0:T(8,128)(2,1)} %get-tuple-element.20), channel_id=1, source_target_pairs={{0,16},{8,24},{16,0},{24,8},{1,17},{9,25},{17,1},{25,9},{2,18},{10... | collective-permute-start | bytes 442376 | tf_op jit(solution)/shard_map/ppermute | solution.py:32
  10.3 2.6 %collective-permute-start.2 = (bf16[288,256]{1,0:T(8,128)(2,1)}, bf16[288,256]{1,0:T(8,128)(2,1)S(1)}, u32[]{:S(2)}, u32[]{:S(2)}) collective-permute-start(bf16[288,256]{1,0:T(8,128)(2,1)} %get-tuple-element.20), channel_id=1, source_target_pairs={{0,8},{8,16},{16,24},{24,0},{1,9},{9,17},{17,25},{25,1},{2,10},{10... | collective-permute-start | bytes 442376 | tf_op jit(solution)/shard_map/ppermute | solution.py:32
  12.9 14.9 %all-to-all-start = ((bf16[16,6,256]{2,1,0:T(8,128)(2,1)}), bf16[16,6,256]{2,1,0:T(8,128)(2,1)S(1)}, u32[]{:S(2)}, u32[]{:S(2)}) async-start(bf16[16,6,256]{2,1,0:T(8,128)(2,1)} %get-tuple-element.19), calls=%async_computation | async-start | bytes 131072 | tf_op jit(solution)/shard_map/all_to_all | solution.py:18
  28.8 1.0 pad_maximum_fusion.1
  30.0 9.4 %all-to-all-done = bf16[16,6,256]{2,1,0:T(8,128)(2,1)S(1)} async-done(((bf16[16,6,256]{2,1,0:T(8,128)(2,1)}), bf16[16,6,256]{2,1,0:T(8,128)(2,1)S(1)}, u32[]{:S(2)}, u32[]{:S(2)}) %all-to-all-start) | async-done | bytes 49184 | tf_op jit(solution)/shard_map/all_to_all | solution.py:18
  43.9 7.4 %all-to-all-start.1 = ((bf16[8,264,96]{2,1,0:T(8,128)(2,1)}), bf16[8,264,96]{2,1,0:T(8,128)(2,1)S(1)}, u32[]{:S(2)}, u32[]{:S(2)}) async-start(bf16[8,264,96]{2,1,0:T(8,128)(2,1)} %constant_dynamic-update-slice_fusion), calls=%async_computation.1 | async-start | bytes 1081344 | tf_op jit(solution)/shard_map/all_to_all | solution.py:18
  51.3 3.6 %collective-permute-start.3 = (bf16[416,256]{1,0:T(8,128)(2,1)S(1)}, bf16[416,256]{1,0:T(8,128)(2,1)S(1)}, u32[]{:S(2)}, u32[]{:S(2)}) collective-permute-start(bf16[416,256]{1,0:T(8,128)(2,1)S(1)} %copy-done.3), channel_id=1, source_target_pairs={{0,16},{8,24},{16,0},{24,8},{1,17},{9,25},{17,1},{25,9},{2,18},{10... | collective-permute-start | bytes 638984 | tf_op jit(solution)/shard_map/ppermute | solution.py:87
  54.9 6.6 %collective-permute-done.3 = bf16[416,256]{1,0:T(8,128)(2,1)S(1)} collective-permute-done((bf16[416,256]{1,0:T(8,128)(2,1)S(1)}, bf16[416,256]{1,0:T(8,128)(2,1)S(1)}, u32[]{:S(2)}, u32[]{:S(2)}) %collective-permute-start.3) | collective-permute-done | bytes 213024 | tf_op jit(solution)/shard_map/ppermute | solution.py:87
  61.5 3.5 %collective-permute-start.4 = (bf16[832,256]{1,0:T(8,128)(2,1)S(1)}, bf16[832,256]{1,0:T(8,128)(2,1)S(1)}, u32[]{:S(2)}, u32[]{:S(2)}) collective-permute-start(bf16[832,256]{1,0:T(8,128)(2,1)S(1)} %pad_maximum_fusion.2), channel_id=1, source_target_pairs={{0,8},{8,0},{16,24},{24,16},{1,9},{9,1},{17,25},{25,17},{2,10},{10... | collective-permute-start | bytes 1277960 | tf_op jit(solution)/shard_map/ppermute | solution.py:87
  65.8 5.6 %all-to-all-start.2 = ((bf16[8,48,96]{2,1,0:T(8,128)(2,1)}), bf16[8,48,96]{2,1,0:T(8,128)(2,1)S(1)}, u32[]{:S(2)}, u32[]{:S(2)}) async-start(bf16[8,48,96]{2,1,0:T(8,128)(2,1)} %broadcast_in_dim.27), calls=%async_computation.2 | async-start | bytes 196608 | tf_op jit(solution)/shard_map/all_to_all | solution.py:18
  71.4 4.9 %all-to-all-done.2 = bf16[8,48,96]{2,1,0:T(8,128)(2,1)S(1)} async-done(((bf16[8,48,96]{2,1,0:T(8,128)(2,1)}), bf16[8,48,96]{2,1,0:T(8,128)(2,1)S(1)}, u32[]{:S(2)}, u32[]{:S(2)}) %all-to-all-start.2) | async-done | bytes 73760 | tf_op jit(solution)/shard_map/all_to_all | solution.py:18
  78.0 3.5 %all-to-all-start.3 = ((bf16[16,16,96]{2,1,0:T(8,128)(2,1)}), bf16[16,16,96]{2,1,0:T(8,128)(2,1)S(1)}, u32[]{:S(2)}, u32[]{:S(2)}) async-start(bf16[16,16,96]{2,1,0:T(8,128)(2,1)} %bitcast.38), calls=%async_computation.3 | async-start | bytes 131072 | tf_op jit(solution)/shard_map/all_to_all | solution.py:18
  81.7 11.4 %all-to-all-done.3 = bf16[16,16,96]{2,1,0:T(8,128)(2,1)S(1)} async-done(((bf16[16,16,96]{2,1,0:T(8,128)(2,1)}), bf16[16,16,96]{2,1,0:T(8,128)(2,1)S(1)}, u32[]{:S(2)}, u32[]{:S(2)}) %all-to-all-start.3) | async-done | bytes 49184 | tf_op jit(solution)/shard_map/all_to_all | solution.py:18
  93.8 5.3 %all-to-all-start.4 = ((bf16[8,16,96]{2,1,0:T(8,128)(2,1)}), bf16[8,16,96]{2,1,0:T(8,128)(2,1)S(1)}, u32[]{:S(2)}, u32[]{:S(2)}) async-start(bf16[8,16,96]{2,1,0:T(8,128)(2,1)} %broadcast_in_dim.28), calls=%async_computation.4 | async-start | bytes 65536 | tf_op jit(solution)/shard_map/all_to_all | solution.py:18
  99.1 4.7 %all-to-all-done.4 = bf16[8,16,96]{2,1,0:T(8,128)(2,1)S(1)} async-done(((bf16[8,16,96]{2,1,0:T(8,128)(2,1)}), bf16[8,16,96]{2,1,0:T(8,128)(2,1)S(1)}, u32[]{:S(2)}, u32[]{:S(2)}) %all-to-all-start.4) | async-done | bytes 24608 | tf_op jit(solution)/shard_map/all_to_all | solution.py:18
  105.6 3.5 %all-to-all-start.5 = ((bf16[16,54,128]{2,1,0:T(8,128)(2,1)}), bf16[16,54,128]{2,1,0:T(8,128)(2,1)S(1)}, u32[]{:S(2)}, u32[]{:S(2)}) async-start(bf16[16,54,128]{2,1,0:T(8,128)(2,1)} %copy.131), calls=%async_computation.5 | async-start | bytes 458752 | tf_op jit(solution)/shard_map/all_to_all | solution.py:18
  109.2 13.2 %all-to-all-done.5 = bf16[16,54,128]{2,1,0:T(8,128)(2,1)S(1)} async-done(((bf16[16,54,128]{2,1,0:T(8,128)(2,1)}), bf16[16,54,128]{2,1,0:T(8,128)(2,1)S(1)}, u32[]{:S(2)}, u32[]{:S(2)}) %all-to-all-start.5) | async-done | bytes 221216 | tf_op jit(solution)/shard_map/all_to_all | solution.py:18
  124.7 11.6 %all_to_all.55 = bf16[8,6,256]{2,1,0:T(8,128)(2,1)S(1)} all-to-all(bf16[8,6,256]{2,1,0:T(8,128)(2,1)S(1)} %bitcast.213), channel_id=1, replica_groups=mesh['z'=16,'y'=4,'x'=4,'c'=2] {'x','c'}, dimensions={0} | all-to-all | bytes 49152 | tf_op jit(solution)/shard_map/all_to_all | solution.py:18
  136.3 17.0 %all_to_all.56 = bf16[16,6,256]{2,1,0:T(8,128)(2,1)S(1)} all-to-all(bf16[16,6,256]{2,1,0:T(8,128)(2,1)S(1)} %broadcast_in_dim.53), channel_id=1, replica_groups=mesh['z'=16,'y'=4,'x'=4,'c'=2] {'z'}, dimensions={0} | all-to-all | bytes 98304 | tf_op jit(solution)/shard_map/all_to_all | solution.py:18
  154.4 10.4 %all_to_all.57 = bf16[8,104,96]{1,2,0:T(8,128)(2,1)S(1)} all-to-all(bf16[8,104,96]{1,2,0:T(8,128)(2,1)S(1)} %copy.139), channel_id=1, replica_groups=mesh['z'=16,'y'=4,'x'=4,'c'=2] {'x','c'}, dimensions={0} | all-to-all | bytes 319488 | tf_op jit(solution)/shard_map/all_to_all | solution.py:18
  165.4 8.3 %all_to_all.58 = bf16[8,48,96]{2,1,0:T(8,128)(2,1)S(1)} all-to-all(bf16[8,48,96]{2,1,0:T(8,128)(2,1)S(1)} %broadcast_in_dim.55), channel_id=1, replica_groups=mesh['z'=16,'y'=4,'x'=4,'c'=2] {'x','c'}, dimensions={0} | all-to-all | bytes 147456 | tf_op jit(solution)/shard_map/all_to_all | solution.py:18
  174.0 14.3 %all_to_all.59 = bf16[16,6,256]{2,1,0:T(8,128)(2,1)S(1)} all-to-all(bf16[16,6,256]{2,1,0:T(8,128)(2,1)S(1)} %reshape.255), channel_id=1, replica_groups=mesh['z'=16,'y'=4,'x'=4,'c'=2] {'z'}, dimensions={0} | all-to-all | bytes 98304 | tf_op jit(solution)/shard_map/all_to_all | solution.py:18
  (134 shorter events, 15.1 us)
Async XLA Ops:
  0.6 123.8 %copy-start = (bf16[256,2048]{1,0:T(8,128)(2,1)S(1)}, bf16[256,2048]{1,0:T(8,128)(2,1)}, u32[]{:S(2)}) copy-start(bf16[256,2048]{1,0:T(8,128)(2,1)} %param.30) | copy-start | bytes 3145732
  2.6 26.2 %collective-permute-start = (bf16[288,256]{1,0:T(8,128)(2,1)}, bf16[288,256]{1,0:T(8,128)(2,1)S(1)}, u32[]{:S(2)}, u32[]{:S(2)}) collective-permute-start(bf16[288,256]{1,0:T(8,128)(2,1)} %get-tuple-element.20), channel_id=1, source_target_pairs={{0,24},{8,0},{16,8},{24,16},{1,25},{9,1},{17,9},{25,17},{2,26},{10... | collective-permute-start | bytes 442376 | tf_op jit(solution)/shard_map/ppermute | solution.py:32
  8.1 20.8 %collective-permute-start.1 = (bf16[288,256]{1,0:T(8,128)(2,1)}, bf16[288,256]{1,0:T(8,128)(2,1)S(1)}, u32[]{:S(2)}, u32[]{:S(2)}) collective-permute-start(bf16[288,256]{1,0:T(8,128)(2,1)} %get-tuple-element.20), channel_id=1, source_target_pairs={{0,16},{8,24},{16,0},{24,8},{1,17},{9,25},{17,1},{25,9},{2,18},{10... | collective-permute-start | bytes 442376 | tf_op jit(solution)/shard_map/ppermute | solution.py:32
  10.3 18.5 %collective-permute-start.2 = (bf16[288,256]{1,0:T(8,128)(2,1)}, bf16[288,256]{1,0:T(8,128)(2,1)S(1)}, u32[]{:S(2)}, u32[]{:S(2)}) collective-permute-start(bf16[288,256]{1,0:T(8,128)(2,1)} %get-tuple-element.20), channel_id=1, source_target_pairs={{0,8},{8,16},{16,24},{24,0},{1,9},{9,17},{17,25},{25,1},{2,10},{10... | collective-permute-start | bytes 442376 | tf_op jit(solution)/shard_map/ppermute | solution.py:32
  12.9 26.5 %all-to-all-start = ((bf16[16,6,256]{2,1,0:T(8,128)(2,1)}), bf16[16,6,256]{2,1,0:T(8,128)(2,1)S(1)}, u32[]{:S(2)}, u32[]{:S(2)}) async-start(bf16[16,6,256]{2,1,0:T(8,128)(2,1)} %get-tuple-element.19), calls=%async_computation | async-start | bytes 131072 | tf_op jit(solution)/shard_map/all_to_all | solution.py:18
  28.8 10.6 %copy-start.6 = (f32[2,128]{1,0:T(2,128)S(1)}, f32[2,128]{1,0:T(2,128)}, u32[]{:S(2)}) copy-start(f32[2,128]{1,0:T(2,128)} %get-tuple-element.24) | copy-start | bytes 3076
  41.2 10.1 %copy-start.3 = (bf16[416,256]{1,0:T(8,128)(2,1)S(1)}, bf16[416,256]{1,0:T(8,128)(2,1)}, u32[]{:S(2)}) copy-start(bf16[416,256]{1,0:T(8,128)(2,1)} %get-tuple-element.26) | copy-start | bytes 638980
  43.9 21.1 %all-to-all-start.1 = ((bf16[8,264,96]{2,1,0:T(8,128)(2,1)}), bf16[8,264,96]{2,1,0:T(8,128)(2,1)S(1)}, u32[]{:S(2)}, u32[]{:S(2)}) async-start(bf16[8,264,96]{2,1,0:T(8,128)(2,1)} %constant_dynamic-update-slice_fusion), calls=%async_computation.1 | async-start | bytes 1081344 | tf_op jit(solution)/shard_map/all_to_all | solution.py:18
  51.3 10.2 %collective-permute-start.3 = (bf16[416,256]{1,0:T(8,128)(2,1)S(1)}, bf16[416,256]{1,0:T(8,128)(2,1)S(1)}, u32[]{:S(2)}, u32[]{:S(2)}) collective-permute-start(bf16[416,256]{1,0:T(8,128)(2,1)S(1)} %copy-done.3), channel_id=1, source_target_pairs={{0,16},{8,24},{16,0},{24,8},{1,17},{9,25},{17,1},{25,9},{2,18},{10... | collective-permute-start | bytes 638984 | tf_op jit(solution)/shard_map/ppermute | solution.py:87
  61.5 20.0 %collective-permute-start.4 = (bf16[832,256]{1,0:T(8,128)(2,1)S(1)}, bf16[832,256]{1,0:T(8,128)(2,1)S(1)}, u32[]{:S(2)}, u32[]{:S(2)}) collective-permute-start(bf16[832,256]{1,0:T(8,128)(2,1)S(1)} %pad_maximum_fusion.2), channel_id=1, source_target_pairs={{0,8},{8,0},{16,24},{24,16},{1,9},{9,1},{17,25},{25,17},{2,10},{10... | collective-permute-start | bytes 1277960 | tf_op jit(solution)/shard_map/ppermute | solution.py:87
  65.0 11.6 %copy-start.2 = (bf16[8,264,96]{2,1,0:T(8,128)(2,1)}, bf16[8,264,96]{2,1,0:T(8,128)(2,1)S(1)}, u32[]{:S(2)}) copy-start(bf16[8,264,96]{2,1,0:T(8,128)(2,1)S(1)} %all-to-all-done.1) | copy-start | bytes 1216516
  65.8 10.5 %all-to-all-start.2 = ((bf16[8,48,96]{2,1,0:T(8,128)(2,1)}), bf16[8,48,96]{2,1,0:T(8,128)(2,1)S(1)}, u32[]{:S(2)}, u32[]{:S(2)}) async-start(bf16[8,48,96]{2,1,0:T(8,128)(2,1)} %broadcast_in_dim.27), calls=%async_computation.2 | async-start | bytes 196608 | tf_op jit(solution)/shard_map/all_to_all | solution.py:18
  78.0 15.1 %all-to-all-start.3 = ((bf16[16,16,96]{2,1,0:T(8,128)(2,1)}), bf16[16,16,96]{2,1,0:T(8,128)(2,1)S(1)}, u32[]{:S(2)}, u32[]{:S(2)}) async-start(bf16[16,16,96]{2,1,0:T(8,128)(2,1)} %bitcast.38), calls=%async_computation.3 | async-start | bytes 131072 | tf_op jit(solution)/shard_map/all_to_all | solution.py:18
  81.6 11.6 %slice-start = ((bf16[8,264,96]{2,1,0:T(8,128)(2,1)}), bf16[8,32,96]{2,1,0:T(8,128)(2,1)S(1)}, s32[]{:S(2)}) async-start(bf16[8,264,96]{2,1,0:T(8,128)(2,1)} %copy-done.2), calls=%async_computation.11 | async-start | bytes 131072 | tf_op jit(solution)/shard_map/slice | solution.py:185
  93.8 10.0 %all-to-all-start.4 = ((bf16[8,16,96]{2,1,0:T(8,128)(2,1)}), bf16[8,16,96]{2,1,0:T(8,128)(2,1)S(1)}, u32[]{:S(2)}, u32[]{:S(2)}) async-start(bf16[8,16,96]{2,1,0:T(8,128)(2,1)} %broadcast_in_dim.28), calls=%async_computation.4 | async-start | bytes 65536 | tf_op jit(solution)/shard_map/all_to_all | solution.py:18
  104.3 4.9 %copy-start.7 = (f32[2,128]{1,0:T(2,128)S(1)}, f32[2,128]{1,0:T(2,128)}, u32[]{:S(2)}) copy-start(f32[2,128]{1,0:T(2,128)} %get-tuple-element.30) | copy-start | bytes 3076
  104.5 18.6 %copy-start.4 = (f32[6,2,128,128]{3,2,1,0:T(8,128)S(1)}, f32[6,2,128,128]{3,2,1,0:T(8,128)}, u32[]{:S(2)}) copy-start(f32[6,2,128,128]{3,2,1,0:T(8,128)} %param.35) | copy-start | bytes 2359300
  105.6 16.8 %all-to-all-start.5 = ((bf16[16,54,128]{2,1,0:T(8,128)(2,1)}), bf16[16,54,128]{2,1,0:T(8,128)(2,1)S(1)}, u32[]{:S(2)}, u32[]{:S(2)}) async-start(bf16[16,54,128]{2,1,0:T(8,128)(2,1)} %copy.131), calls=%async_computation.5 | async-start | bytes 458752 | tf_op jit(solution)/shard_map/all_to_all | solution.py:18
  123.0 1.4 copy-start.8
  123.5 12.8 %copy-start.1 = (f32[6,2,128,128]{3,2,1,0:T(8,128)}, f32[6,2,128,128]{3,2,1,0:T(8,128)S(1)}, u32[]{:S(2)}) copy-start(f32[6,2,128,128]{3,2,1,0:T(8,128)S(1)} %multiply_add_fusion) | copy-start | bytes 2359300
  123.5 29.8 %copy-start.5 = (f32[2,128]{1,0:T(2,128)S(1)}, f32[2,128]{1,0:T(2,128)}, u32[]{:S(2)}) copy-start(f32[2,128]{1,0:T(2,128)} %get-tuple-element.33) | copy-start | bytes 3076

commit v4 on v3

--- a/solution.py
+++ b/solution.py
@@ -87,15 +87,15 @@
     return jnp.concatenate([array, lax.ppermute(array, axis, [(i, i ^ apart) for i in range(n)])])
 
 
-def reordered(blocks, at):
+def reordered(blocks, odd, upper):
     blocks = jnp.stack([blocks[0], blocks[2], blocks[1], blocks[3]])
     halves = jnp.concatenate([blocks[2:], blocks[:2]])
-    blocks = jnp.where(at % 2 == 1, halves, blocks)
+    blocks = jnp.where(odd, halves, blocks)
     pairs = jnp.concatenate([blocks[1:2], blocks[0:1], blocks[3:4], blocks[2:3]])
-    return jnp.where(at // 2 == 1, pairs, blocks)
-
-
-def hidden_units(rows, gain_vec, gate_t, up_t, extra):
+    return jnp.where(upper, pairs, blocks)
+
+
+def hidden_units(rows, gain_vec, gate_t, up_t, extra, finish, later):
     tp = lax.axis_size(TP)
     n = rows.shape[0]
     widened = rows.astype(f32)
@@ -110,12 +110,14 @@
         jnp.broadcast_to(squares.astype(bf16), (tp, 8, n)),
         *extra,
     ]
-    arrived = exchanged(jnp.concatenate(tiles, axis=1), TP)
+    message, *later = lax.optimization_barrier((jnp.concatenate(tiles, axis=1), *later))
+    arrived = exchanged(message, TP)
     summed = arrived[:, : 2 * unit + 8].astype(f32).sum(axis=0)
     inverse = lax.rsqrt(summed[2 * unit] / D + EPSILON)[None, :]
     hidden = (jax.nn.silu(summed[:unit] * inverse) * (summed[unit : 2 * unit] * inverse)).astype(bf16)
+    hidden, *rest = lax.optimization_barrier((hidden, *finish(arrived[:, 2 * unit + 8 :]), *later))
     every = gathered(hidden, TP).reshape(tp * unit, n)
-    return every, arrived[:, 2 * unit + 8 :]
+    return every, rest
 
 
 def shards(
@@ -139,7 +141,7 @@
     memory_state,
 ):
     nz, ny, tp = lax.axis_size("z"), lax.axis_size("y"), lax.axis_size(TP)
-    z_at, t_at = lax.axis_index("z"), lax.axis_index(TP)
+    z_at, t_at, y_at = (lax.axis_index(k).astype(jnp.uint32) for k in ("z", TP, "y"))
     own, width = residual_in.shape
     rows = nz * own
     units = gate_pre.shape[1]
@@ -149,7 +151,6 @@
     halves = width // block
     kept = query_weight.shape[0]
 
-    y_at = lax.axis_index("y")
     spread, first, second, gain_pre, gain_post, head_gain, lower_bound, gain_mix = staged(
         unit,
         nz,
@@ -160,46 +161,53 @@
     )
     gain_pre, gain_post = gain_pre.reshape(width), gain_post.reshape(width)
     gain_block = lax.dynamic_slice_in_dim(gain_mix, z_at * block // HEAD_DIM, block // HEAD_DIM)
-    gain_block = reordered(gain_block.reshape(ny, kept), y_at).reshape(block)
+    gain_block = reordered(gain_block.reshape(ny, kept), y_at % 2 == 1, y_at // 2 == 1).reshape(block)
     first = from_others(first, "y")
+    second = doubled(second, "y", 2)
     all_rows = exchanged(spread, "z")
     first = jnp.stack(first)
     down_tiles = first[:, 2 * unit :].swapaxes(1, 2).reshape(ny, halves, tp, piece, unit)
     down_tiles = down_tiles.transpose(2, 0, 1, 3, 4).reshape(tp, ny * halves * piece, unit)
-    all_rows, first, gain_block, down_tiles = lax.optimization_barrier(
-        (all_rows, first, gain_block, down_tiles)
-    )
+    mine = z_at // halves == t_at
+    elsewhere = (jnp.arange(nz, dtype=jnp.uint32) // halves != t_at)[:, None]
+    note_at = t_at * halves
+    odd, upper = y_at % 2 == 1, y_at // 2 == 1
+    floor_rate = lower_bound.reshape(-1, HEAD_DIM)
+    floors = (jnp.log(floor_rate), jnp.log1p(-floor_rate), 1.0 - floor_rate)
+    all_rows, second, first, down_tiles, *known = lax.optimization_barrier(
+        (all_rows, second, first, down_tiles, gain_block, gain_pre, gain_post, head_gain)
+        + (*floors, mine, elsewhere, note_at, odd, upper, z_at)
+    )
+    gain_block, gain_pre, gain_post, head_gain, log_floor, log_rest, rest_rate = known[:7]
+    mine, elsewhere, note_at, odd, upper, z_at = known[7:]
+    others = lax.ppermute(second, "y", [(i, i ^ 1) for i in range(ny)])
     gate_pre_t = first[:, :unit].reshape(ny * unit, width)
     up_pre_t = first[:, unit : 2 * unit].reshape(ny * unit, width)
 
     all_rows = all_rows.reshape(rows, width)
     turned = all_rows.T.reshape(halves, tp, piece, rows).swapaxes(0, 1)
-    hidden, extra = hidden_units(
+    own_rows = (tp, halves * piece, rows)
+
+    def finish(extra):
+        pieces = extra[:, : halves * piece].reshape(nz, piece, rows)
+        return (
+            lax.dynamic_index_in_dim(pieces, z_at, axis=0, keepdims=False),
+            *[extra[:, k * halves * piece :][:, : halves * piece].reshape(width, unit) for k in range(1, ny + 1)],
+        )
+
+    hidden, (residual, *down_pre_t, second, gain_block) = hidden_units(
         all_rows,
         gain_pre,
         gate_pre_t,
         up_pre_t,
-        (turned.reshape(tp, halves * piece, rows), down_tiles),
-    )
-    residual = lax.dynamic_index_in_dim(
-        extra[:, : halves * piece].reshape(nz, piece, rows), z_at, axis=0, keepdims=False
-    )
-    down_pre_t = extra[:, halves * piece :].reshape(tp, ny, halves * piece, unit)
+        (turned.reshape(own_rows), down_tiles),
+        finish,
+        (second, gain_block),
+    )
     part = sum(
-        dot(
-            down_pre_t[:, k].reshape(width, unit),
-            hidden[k * unit : (k + 1) * unit],
-            1,
-            0,
-        )
-        for k in range(ny)
+        dot(down_pre_t[k], hidden[k * unit : (k + 1) * unit], 1, 0) for k in range(ny)
     ).astype(bf16)
-    second = doubled(second, "y", 2)
-    second = doubled(second, "y", 1).reshape(ny, -1, width)
-    branch = exchanged(part.reshape(nz, piece, rows), "z")
-    branch = branch.astype(f32).sum(axis=0)
-    stream_piece = (residual.astype(f32) + 0.5 * branch).astype(bf16)
-
+    second = jnp.concatenate([second, others]).reshape(ny, -1, width)
     gate_post_t, up_post_t, down_post_all = (
         second[:, k * unit : (k + 1) * unit].reshape(ny * unit, width) for k in range(3)
     )
@@ -210,18 +218,23 @@
         ],
         axis=1,
     )
-    stream_piece, gate_post_t, up_post_t, down_post_all, mixers = lax.optimization_barrier(
-        (stream_piece, gate_post_t, up_post_t, down_post_all, mixers)
-    )
+    part, residual, gate_post_t, up_post_t, down_post_all, mixers, gain_block = (
+        lax.optimization_barrier(
+            (part, residual, gate_post_t, up_post_t, down_post_all, mixers, gain_block)
+        )
+    )
+    branch = exchanged(part.reshape(nz, piece, rows), "z")
+    branch = branch.astype(f32).sum(axis=0)
+    stream_piece = (residual.astype(f32) + 0.5 * branch).astype(bf16)
+
     stream_t = gathered(stream_piece, TP).reshape(block, rows)
     widened = stream_t.astype(f32)
     squares = jnp.sum(widened * widened, axis=0)
-    scaled = reordered(widened.reshape(ny, kept, rows), y_at).reshape(block, rows)
+    scaled = reordered(widened.reshape(ny, kept, rows), odd, upper).reshape(block, rows)
     scaled = (scaled * gain_block[:, None]).astype(bf16)
     heads = width // HEAD_DIM
     parts = dot(scaled, mixers, 0, 0).astype(bf16)
     parts = parts.reshape(nz, own, 4 * heads, HEAD_DIM).swapaxes(1, 2)
-    mine = z_at // halves == t_at
     note = jnp.where(
         mine,
         stream_t.T.reshape(nz, own, block),
@@ -231,9 +244,8 @@
     arrived = exchanged(message, "z")
     projected = arrived[:, : 4 * heads * own].astype(f32).sum(axis=0)
     notes = arrived[:, 4 * heads * own :]
-    stream_a = lax.dynamic_slice_in_dim(notes, t_at * halves, halves, axis=0)
+    stream_a = lax.dynamic_slice_in_dim(notes, note_at, halves, axis=0)
     stream_a = stream_a.swapaxes(0, 1).reshape(own, width).astype(f32)
-    elsewhere = (jnp.arange(nz) // halves != t_at)[:, None]
     total = jnp.sum(jnp.where(elsewhere, notes[:, :, 0].astype(f32), 0.0), axis=0)
     total = total + jnp.sum(stream_a * stream_a, axis=1)
     projected = projected.reshape(4, heads, own, HEAD_DIM)
@@ -242,11 +254,8 @@
     query_pre, forget_pre, value_pre, outgate_pre = (
         projected[k].swapaxes(0, 1) for k in range(4)
     )
-    floor_rate = lower_bound.reshape(heads, HEAD_DIM)
-    log_keep = jnp.logaddexp(
-        jnp.log(floor_rate), jnp.log1p(-floor_rate) + jax.nn.log_sigmoid(forget_pre)
-    )
-    inject = (1.0 - floor_rate) * jax.nn.sigmoid(-forget_pre)
+    log_keep = jnp.logaddexp(log_floor, log_rest + jax.nn.log_sigmoid(forget_pre))
+    inject = rest_rate * jax.nn.sigmoid(-forget_pre)
     next_state = (
         jnp.exp(log_keep)[..., None] * memory_state + inject[..., None] * value_pre[:, :, None, :]
     )
@@ -264,7 +273,7 @@
     stream_b = (stream_a + mixed.astype(f32).sum(axis=0)).astype(bf16)
 
     all_rows = gathered(stream_b, "z").reshape(rows, width)
-    hidden, _ = hidden_units(all_rows, gain_post, gate_post_t, up_post_t, ())
+    hidden, _ = hidden_units(all_rows, gain_post, gate_post_t, up_post_t, (), lambda _: (), ())
     part = dot(hidden, down_post_all, 0, 0).astype(bf16)
     branch = exchanged(part.reshape(nz, own, width), "z").astype(f32).sum(axis=0)
     layer_out = (stream_b.astype(f32) + 0.5 * branch).astype(bf16)

time: 190 us -> 193 us (1.016)
  blocking collectives: 61.6 us -> 126 us
  waiting for transfers between devices: 50.3 us -> 16.6 us
  starting transfers between devices: 57.6 us -> 34.5 us
  local copies, waits for them, and re-layouts: 9.33 us -> 4.08 us
    all_to_all x5 -> x9, blocking collectives: 61.6 us -> 126 us  [exchanged(): return lax.all_to_all(tiles, axis, split_axis=0, concat_axis=0, tiled=True)]
    all_to_all x6 -> x2, waiting for transfers between devices: 43.7 us -> 5.61 us  [exchanged(): return lax.all_to_all(tiles, axis, split_axis=0, concat_axis=0, tiled=True)]
    all_to_all x6 -> x2, starting transfers between devices: 40.2 us -> 18.7 us  [exchanged(): return lax.all_to_all(tiles, axis, split_axis=0, concat_axis=0, tiled=True)]
    ppermute x0 -> x1, waiting for transfers between devices: none -> 7.28 us  [shards(): others = lax.ppermute(second, 'y', [(i, i ^ 1) for i in range(ny)])]
    ppermute x2 -> x1, starting transfers between devices: 7.1 us -> 2.03 us  [doubled(): lax.ppermute(array, axis, [(i, i ^ apart) for i in range(n)])]
    ppermute x2 -> x1, waiting for transfers between devices: 6.59 us -> 3.69 us  [doubled(): lax.ppermute(array, axis, [(i, i ^ apart) for i in range(n)])]
    unnamed x27 -> x23, local copies, waits for them, and re-layouts: 3.02 us -> 0.48 us
    ppermute x0 -> x1, starting transfers between devices: none -> 2.29 us  [shards(): others = lax.ppermute(second, 'y', [(i, i ^ 1) for i in range(ny)])]
  transfers between devices with their start and end apart: 11 -> 7, of which waited for: 6 -> 4; matrix products, arithmetic and copies ran while one was open for 2% -> 2% of each run, Pallas kernels for 0% -> 0%
where the time goes in v4:
time: 193 us; the launch traced here: 192 us
  blocking collectives  126 us (65%)
  starting transfers between devices  34.5 us (18%)
  waiting for transfers between devices  16.6 us (9%)
  other arithmetic  4.27 us (2%)
  local copies, waits for them, and re-layouts  4.08 us (2%)
  matrix products  3.11 us (2%)
  Pallas kernels  1.93 us (1%)
    all_to_all x9, blocking collectives, exchanged(): return lax.all_to_all(tiles, axis, split_axis=0, concat_axis=0, tiled=True)  126 us
    all_to_all x2, starting transfers between devices, exchanged(): return lax.all_to_all(tiles, axis, split_axis=0, concat_axis=0, tiled=True)  18.7 us
    ppermute x3, starting transfers between devices, from_others(): lax.ppermute(array, axis, [(i, (i - k) % n) for i in range(n)])  11.5 us
    ppermute x1, waiting for transfers between devices, shards(): others = lax.ppermute(second, 'y', [(i, i ^ 1) for i in range(ny)])  7.28 us
    all_to_all x2, waiting for transfers between devices, exchanged(): return lax.all_to_all(tiles, axis, split_axis=0, concat_axis=0, tiled=True)  5.61 us
  transfers between devices with their start and end apart: 7, of which 4 were waited for; matrix products, arithmetic and copies ran while one was open for 2% of the time, Pallas kernels for 0%

profile of v4, /device:TPU:1, one launch (start us, length us, event | category | flops | bytes accessed | tf_op | source)
XLA Modules:
  0.0 191.9 jit_solution(13041074201980806378)
XLA Ops:
  0.7 1.9 %shard_map.185 = (bf16[16,6,256]{2,1,0:T(8,128)(2,1)}, bf16[288,256]{1,0:T(8,128)(2,1)}, bf16[416,256]{1,0:T(8,128)(2,1)}, f32[2,128]{1,0:T(2,128)}, f32[2,128]{...) custom-call(bf16[6,256]{1,0:T(8,128)(2,1)} %refs_0_.1, bf16[88,256]{1,0:T(8,128)(2,1)} %bitcast.217, ...), custom_call_target="tpu_custom_call" | custom-call | tf_op jit(solution)/shard_map/pallas_call | solution.py:76
  2.6 4.0 %collective-permute-start.3 = (bf16[288,256]{1,0:T(8,128)(2,1)}, bf16[288,256]{1,0:T(8,128)(2,1)S(1)}, u32[]{:S(2)}, u32[]{:S(2)}) collective-permute-start(bf16[288,256]{1,0:T(8,128)(2,1)} %get-tuple-element.47), channel_id=1, source_target_pairs={{0,8},{8,16},{16,24},{24,0},{1,9},{9,17},{17,25},{25,1},{2,10},{10... | collective-permute-start | bytes 442376 | tf_op jit(solution)/shard_map/ppermute | solution.py:32
  6.6 4.5 %collective-permute-start.2 = (bf16[288,256]{1,0:T(8,128)(2,1)}, bf16[288,256]{1,0:T(8,128)(2,1)S(1)}, u32[]{:S(2)}, u32[]{:S(2)}) collective-permute-start(bf16[288,256]{1,0:T(8,128)(2,1)} %get-tuple-element.47), channel_id=1, source_target_pairs={{0,16},{8,24},{16,0},{24,8},{1,17},{9,25},{17,1},{25,9},{2,18},{10... | collective-permute-start | bytes 442376 | tf_op jit(solution)/shard_map/ppermute | solution.py:32
  11.2 3.0 %collective-permute-start.1 = (bf16[288,256]{1,0:T(8,128)(2,1)}, bf16[288,256]{1,0:T(8,128)(2,1)S(1)}, u32[]{:S(2)}, u32[]{:S(2)}) collective-permute-start(bf16[288,256]{1,0:T(8,128)(2,1)} %get-tuple-element.47), channel_id=1, source_target_pairs={{0,24},{8,0},{16,8},{24,16},{1,25},{9,1},{17,9},{25,17},{2,26},{10... | collective-permute-start | bytes 442376 | tf_op jit(solution)/shard_map/ppermute | solution.py:32
  14.1 14.9 %all-to-all-start = ((bf16[16,6,256]{2,1,0:T(8,128)(2,1)}), bf16[16,6,256]{2,1,0:T(8,128)(2,1)S(1)}, u32[]{:S(2)}, u32[]{:S(2)}) async-start(bf16[16,6,256]{2,1,0:T(8,128)(2,1)} %get-tuple-element.45), calls=%async_computation | async-start | bytes 131072 | tf_op jit(solution)/shard_map/all_to_all | solution.py:18
  29.1 2.0 %collective-permute-start = (bf16[416,256]{1,0:T(8,128)(2,1)}, bf16[416,256]{1,0:T(8,128)(2,1)S(1)}, u32[]{:S(2)}, u32[]{:S(2)}) collective-permute-start(bf16[416,256]{1,0:T(8,128)(2,1)} %get-tuple-element.46), channel_id=1, source_target_pairs={{0,16},{8,24},{16,0},{24,8},{1,17},{9,25},{17,1},{25,9},{2,18},{10... | collective-permute-start | bytes 638984 | tf_op jit(solution)/shard_map/ppermute | solution.py:87
  31.1 0.7 constant_dynamic-slice_fusion
  32.7 1.0 pad_maximum_fusion.1
  34.0 3.7 %collective-permute-done = bf16[416,256]{1,0:T(8,128)(2,1)S(1)} collective-permute-done((bf16[416,256]{1,0:T(8,128)(2,1)}, bf16[416,256]{1,0:T(8,128)(2,1)S(1)}, u32[]{:S(2)}, u32[]{:S(2)}) %collective-permute-start) | collective-permute-done | bytes 213024 | tf_op jit(solution)/shard_map/ppermute | solution.py:87
  37.7 2.9 %all-to-all-done = bf16[16,6,256]{2,1,0:T(8,128)(2,1)S(1)} async-done(((bf16[16,6,256]{2,1,0:T(8,128)(2,1)}), bf16[16,6,256]{2,1,0:T(8,128)(2,1)S(1)}, u32[]{:S(2)}, u32[]{:S(2)}) %all-to-all-start) | async-done | bytes 49184 | tf_op jit(solution)/shard_map/all_to_all | solution.py:18
  41.9 17.2 %all_to_all.55 = bf16[8,264,96]{2,1,0:T(8,128)(2,1)S(1)} all-to-all(bf16[8,264,96]{2,1,0:T(8,128)(2,1)S(1)} %constant_dynamic-update-slice_fusion), channel_id=1, replica_groups=mesh['z'=16,'y'=4,'x'=4,'c'=2] {'x','c'}, dimensions={0} | all-to-all | bytes 811008 | tf_op jit(solution)/shard_map/all_to_all | solution.py:18
  59.9 3.7 %all-to-all-start.2 = ((bf16[8,48,96]{2,1,0:T(8,128)(2,1)}), bf16[8,48,96]{2,1,0:T(8,128)(2,1)S(1)}, u32[]{:S(2)}, u32[]{:S(2)}) async-start(bf16[8,48,96]{2,1,0:T(8,128)(2,1)} %broadcast_in_dim.29), calls=%async_computation.2 | async-start | bytes 196608 | tf_op jit(solution)/shard_map/all_to_all | solution.py:18
  63.6 2.3 %collective-permute-start.4 = (bf16[832,256]{1,0:T(8,128)(2,1)S(1)}, bf16[832,256]{1,0:T(8,128)(2,1)S(1)}, u32[]{:S(2)}, u32[]{:S(2)}) collective-permute-start(bf16[832,256]{1,0:T(8,128)(2,1)S(1)} %pad_maximum_fusion.2), channel_id=1, source_target_pairs={{0,8},{8,0},{16,24},{24,16},{1,9},{9,1},{17,25},{25,17},{2,10},{10... | collective-permute-start | bytes 1277960 | tf_op jit(solution)/shard_map/ppermute | solution.py:183
  65.9 2.7 %all-to-all-done.2 = bf16[8,48,96]{2,1,0:T(8,128)(2,1)S(1)} async-done(((bf16[8,48,96]{2,1,0:T(8,128)(2,1)}), bf16[8,48,96]{2,1,0:T(8,128)(2,1)S(1)}, u32[]{:S(2)}, u32[]{:S(2)}) %all-to-all-start.2) | async-done | bytes 73760 | tf_op jit(solution)/shard_map/all_to_all | solution.py:18
  69.5 7.3 %collective-permute-done.4 = bf16[832,256]{1,0:T(8,128)(2,1)S(1)} collective-permute-done((bf16[832,256]{1,0:T(8,128)(2,1)S(1)}, bf16[832,256]{1,0:T(8,128)(2,1)S(1)}, u32[]{:S(2)}, u32[]{:S(2)}) %collective-permute-start.4) | collective-permute-done | bytes 426016 | tf_op jit(solution)/shard_map/ppermute | solution.py:183
  77.1 19.8 %all_to_all.56 = bf16[16,16,96]{2,1,0:T(8,128)(2,1)S(1)} all-to-all(bf16[16,16,96]{2,1,0:T(8,128)(2,1)S(1)} %bitcast.197), channel_id=1, replica_groups=mesh['z'=16,'y'=4,'x'=4,'c'=2] {'z'}, dimensions={0} | all-to-all | bytes 98304 | tf_op jit(solution)/shard_map/all_to_all | solution.py:18
  96.9 11.5 %all_to_all.57 = bf16[8,16,96]{2,1,0:T(8,128)(2,1)S(1)} all-to-all(bf16[8,16,96]{2,1,0:T(8,128)(2,1)S(1)} %broadcast_in_dim.30), channel_id=1, replica_groups=mesh['z'=16,'y'=4,'x'=4,'c'=2] {'x','c'}, dimensions={0} | all-to-all | bytes 49152 | tf_op jit(solution)/shard_map/all_to_all | solution.py:18
  109.5 16.0 %all_to_all.58 = bf16[16,54,128]{2,1,0:T(8,128)(2,1)S(1)} all-to-all(bf16[16,54,128]{2,1,0:T(8,128)(2,1)S(1)} %copy.131), channel_id=1, replica_groups=mesh['z'=16,'y'=4,'x'=4,'c'=2] {'z'}, dimensions={0} | all-to-all | bytes 442368 | tf_op jit(solution)/shard_map/all_to_all | solution.py:18
  126.6 0.8 fusion.21
  127.8 11.9 %all_to_all.59 = bf16[8,6,256]{2,1,0:T(8,128)(2,1)S(1)} all-to-all(bf16[8,6,256]{2,1,0:T(8,128)(2,1)S(1)} %bitcast.211), channel_id=1, replica_groups=mesh['z'=16,'y'=4,'x'=4,'c'=2] {'x','c'}, dimensions={0} | all-to-all | bytes 49152 | tf_op jit(solution)/shard_map/all_to_all | solution.py:18
  139.8 16.6 %all_to_all.60 = bf16[16,6,256]{2,1,0:T(8,128)(2,1)S(1)} all-to-all(bf16[16,6,256]{2,1,0:T(8,128)(2,1)S(1)} %broadcast_in_dim.58), channel_id=1, replica_groups=mesh['z'=16,'y'=4,'x'=4,'c'=2] {'z'}, dimensions={0} | all-to-all | bytes 98304 | tf_op jit(solution)/shard_map/all_to_all | solution.py:18
  157.5 10.4 %all_to_all.61 = bf16[8,104,96]{1,2,0:T(8,128)(2,1)S(1)} all-to-all(bf16[8,104,96]{1,2,0:T(8,128)(2,1)S(1)} %copy.139), channel_id=1, replica_groups=mesh['z'=16,'y'=4,'x'=4,'c'=2] {'x','c'}, dimensions={0} | all-to-all | bytes 319488 | tf_op jit(solution)/shard_map/all_to_all | solution.py:18
  168.5 8.3 %all_to_all.62 = bf16[8,48,96]{2,1,0:T(8,128)(2,1)S(1)} all-to-all(bf16[8,48,96]{2,1,0:T(8,128)(2,1)S(1)} %broadcast_in_dim.60), channel_id=1, replica_groups=mesh['z'=16,'y'=4,'x'=4,'c'=2] {'x','c'}, dimensions={0} | all-to-all | bytes 147456 | tf_op jit(solution)/shard_map/all_to_all | solution.py:18
  177.0 14.3 %all_to_all.63 = bf16[16,6,256]{2,1,0:T(8,128)(2,1)S(1)} all-to-all(bf16[16,6,256]{2,1,0:T(8,128)(2,1)S(1)} %reshape.268), channel_id=1, replica_groups=mesh['z'=16,'y'=4,'x'=4,'c'=2] {'z'}, dimensions={0} | all-to-all | bytes 98304 | tf_op jit(solution)/shard_map/all_to_all | solution.py:18
  (124 shorter events, 9.0 us)
Async XLA Ops:
  0.6 126.9 %copy-start = (bf16[256,2048]{1,0:T(8,128)(2,1)S(1)}, bf16[256,2048]{1,0:T(8,128)(2,1)}, u32[]{:S(2)}) copy-start(bf16[256,2048]{1,0:T(8,128)(2,1)} %param.30) | copy-start | bytes 3145732
  2.6 30.1 %collective-permute-start.3 = (bf16[288,256]{1,0:T(8,128)(2,1)}, bf16[288,256]{1,0:T(8,128)(2,1)S(1)}, u32[]{:S(2)}, u32[]{:S(2)}) collective-permute-start(bf16[288,256]{1,0:T(8,128)(2,1)} %get-tuple-element.47), channel_id=1, source_target_pairs={{0,8},{8,16},{16,24},{24,0},{1,9},{9,17},{17,25},{25,1},{2,10},{10... | collective-permute-start | bytes 442376 | tf_op jit(solution)/shard_map/ppermute | solution.py:32
  6.6 26.1 %collective-permute-start.2 = (bf16[288,256]{1,0:T(8,128)(2,1)}, bf16[288,256]{1,0:T(8,128)(2,1)S(1)}, u32[]{:S(2)}, u32[]{:S(2)}) collective-permute-start(bf16[288,256]{1,0:T(8,128)(2,1)} %get-tuple-element.47), channel_id=1, source_target_pairs={{0,16},{8,24},{16,0},{24,8},{1,17},{9,25},{17,1},{25,9},{2,18},{10... | collective-permute-start | bytes 442376 | tf_op jit(solution)/shard_map/ppermute | solution.py:32
  11.2 21.6 %collective-permute-start.1 = (bf16[288,256]{1,0:T(8,128)(2,1)}, bf16[288,256]{1,0:T(8,128)(2,1)S(1)}, u32[]{:S(2)}, u32[]{:S(2)}) collective-permute-start(bf16[288,256]{1,0:T(8,128)(2,1)} %get-tuple-element.47), channel_id=1, source_target_pairs={{0,24},{8,0},{16,8},{24,16},{1,25},{9,1},{17,9},{25,17},{2,26},{10... | collective-permute-start | bytes 442376 | tf_op jit(solution)/shard_map/ppermute | solution.py:32
  14.1 26.5 %all-to-all-start = ((bf16[16,6,256]{2,1,0:T(8,128)(2,1)}), bf16[16,6,256]{2,1,0:T(8,128)(2,1)S(1)}, u32[]{:S(2)}, u32[]{:S(2)}) async-start(bf16[16,6,256]{2,1,0:T(8,128)(2,1)} %get-tuple-element.45), calls=%async_computation | async-start | bytes 131072 | tf_op jit(solution)/shard_map/all_to_all | solution.py:18
  29.1 8.6 %collective-permute-start = (bf16[416,256]{1,0:T(8,128)(2,1)}, bf16[416,256]{1,0:T(8,128)(2,1)S(1)}, u32[]{:S(2)}, u32[]{:S(2)}) collective-permute-start(bf16[416,256]{1,0:T(8,128)(2,1)} %get-tuple-element.46), channel_id=1, source_target_pairs={{0,16},{8,24},{16,0},{24,8},{1,17},{9,25},{17,1},{25,9},{2,18},{10... | collective-permute-start | bytes 638984 | tf_op jit(solution)/shard_map/ppermute | solution.py:87
  32.7 5.0 %copy-start.3 = (bf16[416,256]{1,0:T(8,128)(2,1)S(1)}, bf16[416,256]{1,0:T(8,128)(2,1)}, u32[]{:S(2)}) copy-start(bf16[416,256]{1,0:T(8,128)(2,1)} %get-tuple-element.46) | copy-start | bytes 638980
  34.0 6.7 %copy-start.5 = (f32[2,128]{1,0:T(2,128)S(1)}, f32[2,128]{1,0:T(2,128)}, u32[]{:S(2)}) copy-start(f32[2,128]{1,0:T(2,128)} %get-tuple-element.49) | copy-start | bytes 3076
  59.9 8.7 %all-to-all-start.2 = ((bf16[8,48,96]{2,1,0:T(8,128)(2,1)}), bf16[8,48,96]{2,1,0:T(8,128)(2,1)S(1)}, u32[]{:S(2)}, u32[]{:S(2)}) async-start(bf16[8,48,96]{2,1,0:T(8,128)(2,1)} %broadcast_in_dim.29), calls=%async_computation.2 | async-start | bytes 196608 | tf_op jit(solution)/shard_map/all_to_all | solution.py:18
  63.6 13.1 %collective-permute-start.4 = (bf16[832,256]{1,0:T(8,128)(2,1)S(1)}, bf16[832,256]{1,0:T(8,128)(2,1)S(1)}, u32[]{:S(2)}, u32[]{:S(2)}) collective-permute-start(bf16[832,256]{1,0:T(8,128)(2,1)S(1)} %pad_maximum_fusion.2), channel_id=1, source_target_pairs={{0,8},{8,0},{16,24},{24,16},{1,9},{9,1},{17,25},{25,17},{2,10},{10... | collective-permute-start | bytes 1277960 | tf_op jit(solution)/shard_map/ppermute | solution.py:183
  109.3 16.9 %copy-start.2 = (f32[6,2,128,128]{3,2,1,0:T(8,128)S(1)}, f32[6,2,128,128]{3,2,1,0:T(8,128)}, u32[]{:S(2)}) copy-start(f32[6,2,128,128]{3,2,1,0:T(8,128)} %param.35) | copy-start | bytes 2359300
  126.1 1.4 copy-start.6
  126.6 13.1 %copy-start.1 = (f32[6,2,128,128]{3,2,1,0:T(8,128)}, f32[6,2,128,128]{3,2,1,0:T(8,128)S(1)}, u32[]{:S(2)}) copy-start(f32[6,2,128,128]{3,2,1,0:T(8,128)S(1)} %multiply_add_fusion) | copy-start | bytes 2359300
  126.6 30.0 %copy-start.4 = (f32[2,128]{1,0:T(2,128)S(1)}, f32[2,128]{1,0:T(2,128)}, u32[]{:S(2)}) copy-start(f32[2,128]{1,0:T(2,128)} %get-tuple-element.50) | copy-start | bytes 3076

commit v5 on v4

--- a/solution.py
+++ b/solution.py
@@ -14,8 +14,10 @@
 bf16 = jnp.bfloat16
 
 
-def exchanged(tiles, axis):
-    return lax.all_to_all(tiles, axis, split_axis=0, concat_axis=0, tiled=True)
+def exchanged(tiles, axis, groups=None):
+    return lax.all_to_all(
+        tiles, axis, split_axis=0, concat_axis=0, axis_index_groups=groups, tiled=True
+    )
 
 
 def gathered(array, axis):
@@ -164,7 +166,9 @@
     gain_block = reordered(gain_block.reshape(ny, kept), y_at % 2 == 1, y_at // 2 == 1).reshape(block)
     first = from_others(first, "y")
     second = doubled(second, "y", 2)
-    all_rows = exchanged(spread, "z")
+    middle = [*range(nz // 2, nz), *range(nz // 2)]
+    all_rows = exchanged(spread, "z", [middle])
+    all_rows = jnp.concatenate([all_rows[nz // 2 :], all_rows[: nz // 2]])
     first = jnp.stack(first)
     down_tiles = first[:, 2 * unit :].swapaxes(1, 2).reshape(ny, halves, tp, piece, unit)
     down_tiles = down_tiles.transpose(2, 0, 1, 3, 4).reshape(tp, ny * halves * piece, unit)

time: 193 us -> 189 us (0.979)
  starting transfers between devices: 34.5 us -> 37.9 us
  waiting for transfers between devices: 16.6 us -> 13.4 us
  blocking collectives: 126 us -> 123 us
    all_to_all x9, blocking collectives: 126 us -> 123 us  [exchanged(): lax.all_to_all(tiles, axis, split_axis=0, concat_axis=0, axis_index_group...]
    all_to_all x2, starting transfers between devices: 18.7 us -> 22.1 us  [exchanged(): lax.all_to_all(tiles, axis, split_axis=0, concat_axis=0, axis_index_group...]
    all_to_all x2, waiting for transfers between devices: 5.61 us -> 2.7 us  [exchanged(): lax.all_to_all(tiles, axis, split_axis=0, concat_axis=0, axis_index_group...]
  transfers between devices with their start and end apart: 7 -> 7, of which waited for: 4 -> 3; matrix products, arithmetic and copies ran while one was open for 2% -> 2% of each run, Pallas kernels for 0% -> 0%
where the time goes in v5:
time: 189 us
  blocking collectives  123 us (65%)
  starting transfers between devices  37.9 us (20%)
  waiting for transfers between devices  13.4 us (7%)
  other arithmetic  4.25 us (2%)
  local copies, waits for them, and re-layouts  4.09 us (2%)
  matrix products  3.12 us (2%)
  Pallas kernels  1.93 us (1%)
    all_to_all x9, blocking collectives, exchanged(): lax.all_to_all(tiles, axis, split_axis=0, concat_axis=0, axis_index_group...  123 us
    all_to_all x2, starting transfers between devices, exchanged(): lax.all_to_all(tiles, axis, split_axis=0, concat_axis=0, axis_index_group...  22.1 us
    ppermute x3, starting transfers between devices, from_others(): lax.ppermute(array, axis, [(i, (i - k) % n) for i in range(n)])  11.5 us
    ppermute x1, waiting for transfers between devices, shards(): others = lax.ppermute(second, 'y', [(i, i ^ 1) for i in range(ny)])  7.28 us
  transfers between devices with their start and end apart: 7, of which 3 were waited for; matrix products, arithmetic and copies ran while one was open for 2% of the time, Pallas kernels for 0%

profile of v5, /device:TPU:1, one launch (start us, length us, event | category | flops | bytes accessed | tf_op | source)
XLA Modules:
  0.0 188.5 jit_solution(11755899130077482098)
XLA Ops:
  0.7 1.9 %shard_map.185 = (bf16[16,6,256]{2,1,0:T(8,128)(2,1)}, bf16[288,256]{1,0:T(8,128)(2,1)}, bf16[416,256]{1,0:T(8,128)(2,1)}, f32[2,128]{1,0:T(2,128)}, f32[2,128]{...) custom-call(bf16[6,256]{1,0:T(8,128)(2,1)} %refs_0_.1, bf16[88,256]{1,0:T(8,128)(2,1)} %bitcast.217, ...), custom_call_target="tpu_custom_call" | custom-call | tf_op jit(solution)/shard_map/pallas_call | solution.py:78
  2.6 4.0 %collective-permute-start.3 = (bf16[288,256]{1,0:T(8,128)(2,1)}, bf16[288,256]{1,0:T(8,128)(2,1)S(1)}, u32[]{:S(2)}, u32[]{:S(2)}) collective-permute-start(bf16[288,256]{1,0:T(8,128)(2,1)} %get-tuple-element.47), channel_id=1, source_target_pairs={{0,8},{8,16},{16,24},{24,0},{1,9},{9,17},{17,25},{25,1},{2,10},{10... | collective-permute-start | bytes 442376 | tf_op jit(solution)/shard_map/ppermute | solution.py:34
  6.6 4.5 %collective-permute-start.2 = (bf16[288,256]{1,0:T(8,128)(2,1)}, bf16[288,256]{1,0:T(8,128)(2,1)S(1)}, u32[]{:S(2)}, u32[]{:S(2)}) collective-permute-start(bf16[288,256]{1,0:T(8,128)(2,1)} %get-tuple-element.47), channel_id=1, source_target_pairs={{0,16},{8,24},{16,0},{24,8},{1,17},{9,25},{17,1},{25,9},{2,18},{10... | collective-permute-start | bytes 442376 | tf_op jit(solution)/shard_map/ppermute | solution.py:34
  11.2 3.0 %collective-permute-start.1 = (bf16[288,256]{1,0:T(8,128)(2,1)}, bf16[288,256]{1,0:T(8,128)(2,1)S(1)}, u32[]{:S(2)}, u32[]{:S(2)}) collective-permute-start(bf16[288,256]{1,0:T(8,128)(2,1)} %get-tuple-element.47), channel_id=1, source_target_pairs={{0,24},{8,0},{16,8},{24,16},{1,25},{9,1},{17,9},{25,17},{2,26},{10... | collective-permute-start | bytes 442376 | tf_op jit(solution)/shard_map/ppermute | solution.py:34
  14.1 18.3 %all-to-all-start = ((bf16[16,6,256]{2,1,0:T(8,128)(2,1)}), bf16[16,6,256]{2,1,0:T(8,128)(2,1)S(1)}, u32[]{:S(2)}, u32[]{:S(2)}) async-start(bf16[16,6,256]{2,1,0:T(8,128)(2,1)} %get-tuple-element.45), calls=%async_computation | async-start | bytes 131072 | tf_op jit(solution)/shard_map/all_to_all | solution.py:18
  32.4 2.0 %collective-permute-start = (bf16[416,256]{1,0:T(8,128)(2,1)}, bf16[416,256]{1,0:T(8,128)(2,1)S(1)}, u32[]{:S(2)}, u32[]{:S(2)}) collective-permute-start(bf16[416,256]{1,0:T(8,128)(2,1)} %get-tuple-element.46), channel_id=1, source_target_pairs={{0,16},{8,24},{16,0},{24,8},{1,17},{9,25},{17,1},{25,9},{2,18},{10... | collective-permute-start | bytes 638984 | tf_op jit(solution)/shard_map/ppermute | solution.py:89
  34.5 0.7 constant_dynamic-slice_fusion
  35.3 0.7 broadcast_subtract_fusion
  36.1 1.0 pad_maximum_fusion.1
  37.4 3.4 %collective-permute-done = bf16[416,256]{1,0:T(8,128)(2,1)S(1)} collective-permute-done((bf16[416,256]{1,0:T(8,128)(2,1)}, bf16[416,256]{1,0:T(8,128)(2,1)S(1)}, u32[]{:S(2)}, u32[]{:S(2)}) %collective-permute-start) | collective-permute-done | bytes 213024 | tf_op jit(solution)/shard_map/ppermute | solution.py:89
  42.0 17.4 %all_to_all.55 = bf16[8,264,96]{2,1,0:T(8,128)(2,1)S(1)} all-to-all(bf16[8,264,96]{2,1,0:T(8,128)(2,1)S(1)} %constant_dynamic-update-slice_fusion), channel_id=1, replica_groups=mesh['z'=16,'y'=4,'x'=4,'c'=2] {'x','c'}, dimensions={0} | all-to-all | bytes 811008 | tf_op jit(solution)/shard_map/all_to_all | solution.py:18
  60.2 3.7 %all-to-all-start.2 = ((bf16[8,48,96]{2,1,0:T(8,128)(2,1)}), bf16[8,48,96]{2,1,0:T(8,128)(2,1)S(1)}, u32[]{:S(2)}, u32[]{:S(2)}) async-start(bf16[8,48,96]{2,1,0:T(8,128)(2,1)} %broadcast_in_dim.29), calls=%async_computation.2 | async-start | bytes 196608 | tf_op jit(solution)/shard_map/all_to_all | solution.py:18
  63.9 2.3 %collective-permute-start.4 = (bf16[832,256]{1,0:T(8,128)(2,1)S(1)}, bf16[832,256]{1,0:T(8,128)(2,1)S(1)}, u32[]{:S(2)}, u32[]{:S(2)}) collective-permute-start(bf16[832,256]{1,0:T(8,128)(2,1)S(1)} %pad_maximum_fusion.2), channel_id=1, source_target_pairs={{0,8},{8,0},{16,24},{24,16},{1,9},{9,1},{17,25},{25,17},{2,10},{10... | collective-permute-start | bytes 1277960 | tf_op jit(solution)/shard_map/ppermute | solution.py:187
  66.2 2.7 %all-to-all-done.2 = bf16[8,48,96]{2,1,0:T(8,128)(2,1)S(1)} async-done(((bf16[8,48,96]{2,1,0:T(8,128)(2,1)}), bf16[8,48,96]{2,1,0:T(8,128)(2,1)S(1)}, u32[]{:S(2)}, u32[]{:S(2)}) %all-to-all-start.2) | async-done | bytes 73760 | tf_op jit(solution)/shard_map/all_to_all | solution.py:18
  69.8 7.3 %collective-permute-done.4 = bf16[832,256]{1,0:T(8,128)(2,1)S(1)} collective-permute-done((bf16[832,256]{1,0:T(8,128)(2,1)S(1)}, bf16[832,256]{1,0:T(8,128)(2,1)S(1)}, u32[]{:S(2)}, u32[]{:S(2)}) %collective-permute-start.4) | collective-permute-done | bytes 426016 | tf_op jit(solution)/shard_map/ppermute | solution.py:187
  77.3 16.1 %all_to_all.56 = bf16[16,16,96]{2,1,0:T(8,128)(2,1)S(1)} all-to-all(bf16[16,16,96]{2,1,0:T(8,128)(2,1)S(1)} %bitcast.197), channel_id=1, replica_groups=mesh['z'=16,'y'=4,'x'=4,'c'=2] {'z'}, dimensions={0} | all-to-all | bytes 98304 | tf_op jit(solution)/shard_map/all_to_all | solution.py:18
  93.5 11.5 %all_to_all.57 = bf16[8,16,96]{2,1,0:T(8,128)(2,1)S(1)} all-to-all(bf16[8,16,96]{2,1,0:T(8,128)(2,1)S(1)} %broadcast_in_dim.30), channel_id=1, replica_groups=mesh['z'=16,'y'=4,'x'=4,'c'=2] {'x','c'}, dimensions={0} | all-to-all | bytes 49152 | tf_op jit(solution)/shard_map/all_to_all | solution.py:18
  106.0 16.0 %all_to_all.58 = bf16[16,54,128]{2,1,0:T(8,128)(2,1)S(1)} all-to-all(bf16[16,54,128]{2,1,0:T(8,128)(2,1)S(1)} %copy.131), channel_id=1, replica_groups=mesh['z'=16,'y'=4,'x'=4,'c'=2] {'z'}, dimensions={0} | all-to-all | bytes 442368 | tf_op jit(solution)/shard_map/all_to_all | solution.py:18
  123.2 0.8 fusion.21
  124.4 11.9 %all_to_all.59 = bf16[8,6,256]{2,1,0:T(8,128)(2,1)S(1)} all-to-all(bf16[8,6,256]{2,1,0:T(8,128)(2,1)S(1)} %bitcast.211), channel_id=1, replica_groups=mesh['z'=16,'y'=4,'x'=4,'c'=2] {'x','c'}, dimensions={0} | all-to-all | bytes 49152 | tf_op jit(solution)/shard_map/all_to_all | solution.py:18
  136.3 16.6 %all_to_all.60 = bf16[16,6,256]{2,1,0:T(8,128)(2,1)S(1)} all-to-all(bf16[16,6,256]{2,1,0:T(8,128)(2,1)S(1)} %broadcast_in_dim.58), channel_id=1, replica_groups=mesh['z'=16,'y'=4,'x'=4,'c'=2] {'z'}, dimensions={0} | all-to-all | bytes 98304 | tf_op jit(solution)/shard_map/all_to_all | solution.py:18
  154.1 10.4 %all_to_all.61 = bf16[8,104,96]{1,2,0:T(8,128)(2,1)S(1)} all-to-all(bf16[8,104,96]{1,2,0:T(8,128)(2,1)S(1)} %copy.139), channel_id=1, replica_groups=mesh['z'=16,'y'=4,'x'=4,'c'=2] {'x','c'}, dimensions={0} | all-to-all | bytes 319488 | tf_op jit(solution)/shard_map/all_to_all | solution.py:18
  165.0 8.3 %all_to_all.62 = bf16[8,48,96]{2,1,0:T(8,128)(2,1)S(1)} all-to-all(bf16[8,48,96]{2,1,0:T(8,128)(2,1)S(1)} %broadcast_in_dim.60), channel_id=1, replica_groups=mesh['z'=16,'y'=4,'x'=4,'c'=2] {'x','c'}, dimensions={0} | all-to-all | bytes 147456 | tf_op jit(solution)/shard_map/all_to_all | solution.py:18
  173.6 14.3 %all_to_all.63 = bf16[16,6,256]{2,1,0:T(8,128)(2,1)S(1)} all-to-all(bf16[16,6,256]{2,1,0:T(8,128)(2,1)S(1)} %reshape.268), channel_id=1, replica_groups=mesh['z'=16,'y'=4,'x'=4,'c'=2] {'z'}, dimensions={0} | all-to-all | bytes 98304 | tf_op jit(solution)/shard_map/all_to_all | solution.py:18
  (126 shorter events, 8.4 us)
Async XLA Ops:
  0.6 123.4 %copy-start = (bf16[256,2048]{1,0:T(8,128)(2,1)S(1)}, bf16[256,2048]{1,0:T(8,128)(2,1)}, u32[]{:S(2)}) copy-start(bf16[256,2048]{1,0:T(8,128)(2,1)} %param.30) | copy-start | bytes 3145732
  2.6 33.5 %collective-permute-start.3 = (bf16[288,256]{1,0:T(8,128)(2,1)}, bf16[288,256]{1,0:T(8,128)(2,1)S(1)}, u32[]{:S(2)}, u32[]{:S(2)}) collective-permute-start(bf16[288,256]{1,0:T(8,128)(2,1)} %get-tuple-element.47), channel_id=1, source_target_pairs={{0,8},{8,16},{16,24},{24,0},{1,9},{9,17},{17,25},{25,1},{2,10},{10... | collective-permute-start | bytes 442376 | tf_op jit(solution)/shard_map/ppermute | solution.py:34
  6.6 29.4 %collective-permute-start.2 = (bf16[288,256]{1,0:T(8,128)(2,1)}, bf16[288,256]{1,0:T(8,128)(2,1)S(1)}, u32[]{:S(2)}, u32[]{:S(2)}) collective-permute-start(bf16[288,256]{1,0:T(8,128)(2,1)} %get-tuple-element.47), channel_id=1, source_target_pairs={{0,16},{8,24},{16,0},{24,8},{1,17},{9,25},{17,1},{25,9},{2,18},{10... | collective-permute-start | bytes 442376 | tf_op jit(solution)/shard_map/ppermute | solution.py:34
  11.2 24.9 %collective-permute-start.1 = (bf16[288,256]{1,0:T(8,128)(2,1)}, bf16[288,256]{1,0:T(8,128)(2,1)S(1)}, u32[]{:S(2)}, u32[]{:S(2)}) collective-permute-start(bf16[288,256]{1,0:T(8,128)(2,1)} %get-tuple-element.47), channel_id=1, source_target_pairs={{0,24},{8,0},{16,8},{24,16},{1,25},{9,1},{17,9},{25,17},{2,26},{10... | collective-permute-start | bytes 442376 | tf_op jit(solution)/shard_map/ppermute | solution.py:34
  14.1 23.2 %all-to-all-start = ((bf16[16,6,256]{2,1,0:T(8,128)(2,1)}), bf16[16,6,256]{2,1,0:T(8,128)(2,1)S(1)}, u32[]{:S(2)}, u32[]{:S(2)}) async-start(bf16[16,6,256]{2,1,0:T(8,128)(2,1)} %get-tuple-element.45), calls=%async_computation | async-start | bytes 131072 | tf_op jit(solution)/shard_map/all_to_all | solution.py:18
  32.4 8.3 %collective-permute-start = (bf16[416,256]{1,0:T(8,128)(2,1)}, bf16[416,256]{1,0:T(8,128)(2,1)S(1)}, u32[]{:S(2)}, u32[]{:S(2)}) collective-permute-start(bf16[416,256]{1,0:T(8,128)(2,1)} %get-tuple-element.46), channel_id=1, source_target_pairs={{0,16},{8,24},{16,0},{24,8},{1,17},{9,25},{17,1},{25,9},{2,18},{10... | collective-permute-start | bytes 638984 | tf_op jit(solution)/shard_map/ppermute | solution.py:89
  37.1 3.7 %copy-start.3 = (bf16[416,256]{1,0:T(8,128)(2,1)S(1)}, bf16[416,256]{1,0:T(8,128)(2,1)}, u32[]{:S(2)}) copy-start(bf16[416,256]{1,0:T(8,128)(2,1)} %get-tuple-element.46) | copy-start | bytes 638980
  37.3 3.5 %copy-start.5 = (f32[2,128]{1,0:T(2,128)S(1)}, f32[2,128]{1,0:T(2,128)}, u32[]{:S(2)}) copy-start(f32[2,128]{1,0:T(2,128)} %get-tuple-element.49) | copy-start | bytes 3076
  60.2 8.7 %all-to-all-start.2 = ((bf16[8,48,96]{2,1,0:T(8,128)(2,1)}), bf16[8,48,96]{2,1,0:T(8,128)(2,1)S(1)}, u32[]{:S(2)}, u32[]{:S(2)}) async-start(bf16[8,48,96]{2,1,0:T(8,128)(2,1)} %broadcast_in_dim.29), calls=%async_computation.2 | async-start | bytes 196608 | tf_op jit(solution)/shard_map/all_to_all | solution.py:18
  63.9 13.1 %collective-permute-start.4 = (bf16[832,256]{1,0:T(8,128)(2,1)S(1)}, bf16[832,256]{1,0:T(8,128)(2,1)S(1)}, u32[]{:S(2)}, u32[]{:S(2)}) collective-permute-start(bf16[832,256]{1,0:T(8,128)(2,1)S(1)} %pad_maximum_fusion.2), channel_id=1, source_target_pairs={{0,8},{8,0},{16,24},{24,16},{1,9},{9,1},{17,25},{25,17},{2,10},{10... | collective-permute-start | bytes 1277960 | tf_op jit(solution)/shard_map/ppermute | solution.py:187
  105.8 16.9 %copy-start.2 = (f32[6,2,128,128]{3,2,1,0:T(8,128)S(1)}, f32[6,2,128,128]{3,2,1,0:T(8,128)}, u32[]{:S(2)}) copy-start(f32[6,2,128,128]{3,2,1,0:T(8,128)} %param.35) | copy-start | bytes 2359300
  122.7 1.4 copy-start.6
  123.2 13.1 %copy-start.1 = (f32[6,2,128,128]{3,2,1,0:T(8,128)}, f32[6,2,128,128]{3,2,1,0:T(8,128)S(1)}, u32[]{:S(2)}) copy-start(f32[6,2,128,128]{3,2,1,0:T(8,128)S(1)} %multiply_add_fusion) | copy-start | bytes 2359300
  123.2 30.0 %copy-start.4 = (f32[2,128]{1,0:T(2,128)S(1)}, f32[2,128]{1,0:T(2,128)}, u32[]{:S(2)}) copy-start(f32[2,128]{1,0:T(2,128)} %get-tuple-element.50) | copy-start | bytes 3076

commit v6 on v5

--- a/solution.py
+++ b/solution.py
@@ -36,16 +36,17 @@
     return [array, *later]
 
 
-def staged(unit, copies, ups, downs, kept, small):
+def staged(unit, copies, at, ups, downs, kept, small, floor_rate, gains):
     rows, gate_a, up_a, down_a, gate_b, up_b, down_b, *projections = ups + downs + kept
     units, width = gate_a.shape
     height = projections[0].shape[0]
-    n_in = 7 + len(projections) + len(small)
-
-    def kernel(*refs):
-        ins, outs = refs[:n_in], refs[n_in : n_in + 3 + len(small)]
-        held, sems = refs[-2], refs[-1]
+    n_in = 9 + len(projections) + len(small)
+
+    def kernel(at_ref, *refs):
+        ins, outs = refs[:n_in], refs[n_in:-4]
+        held, held_floor, held_gains, sems = refs[-4:]
         spread, first, second = outs[:3]
+        gain_block, log_floor, log_rest, rest = outs[3 + len(small) :]
         moves = [(ins[0], held)]
         moves += [(ins[1 + k], first.at[pl.ds(k * unit, units)]) for k in range(3)]
         moves += [(ins[4 + k], second.at[pl.ds(k * unit, units)]) for k in range(3)]
@@ -53,6 +54,7 @@
             moves.append((ins[7 + k], second.at[pl.ds(3 * unit + k * height, height)]))
         for k in range(len(small)):
             moves.append((ins[7 + len(projections) + k], outs[3 + k]))
+        moves += [(ins[-2], held_floor), (ins[-1], held_gains)]
         started = [pltpu.make_async_copy(a, b, sems.at[k]) for k, (a, b) in enumerate(moves)]
         for move in started:
             move.start()
@@ -66,27 +68,36 @@
             spread[k] = held[...]
         for move in started[1:]:
             move.wait()
+        gain_block[...] = held_gains[pl.ds(at_ref[0], 1), :]
+        floor = held_floor[...]
+        log_floor[...] = jnp.log(floor)
+        log_rest[...] = jnp.log1p(-floor)
+        rest[...] = 1.0 - floor
 
     arrays = [rows, gate_a, up_a, down_a, gate_b, up_b, down_b, *projections, *small]
+    arrays += [floor_rate, gains]
     vmem = pl.BlockSpec(memory_space=pltpu.VMEM)
     shapes = [
         jax.ShapeDtypeStruct((copies, *rows.shape), bf16),
         jax.ShapeDtypeStruct((3 * unit, width), bf16),
         jax.ShapeDtypeStruct((3 * unit + len(projections) * height, width), bf16),
         *[jax.ShapeDtypeStruct(v.shape, v.dtype) for v in small],
+        jax.ShapeDtypeStruct((1, gains.shape[1]), f32),
+        *[jax.ShapeDtypeStruct(floor_rate.shape, f32)] * 3,
     ]
     return pl.pallas_call(
         kernel,
         out_shape=shapes,
-        in_specs=[pl.BlockSpec(memory_space=pl.ANY)] * n_in,
+        in_specs=[pl.BlockSpec(memory_space=pltpu.SMEM)]
+        + [pl.BlockSpec(memory_space=pl.ANY)] * n_in,
         out_specs=[vmem] * len(shapes),
-        scratch_shapes=[pltpu.VMEM(rows.shape, bf16), pltpu.SemaphoreType.DMA((n_in,))],
-    )(*arrays)
-
-
-def doubled(array, axis, apart):
-    n = lax.axis_size(axis)
-    return jnp.concatenate([array, lax.ppermute(array, axis, [(i, i ^ apart) for i in range(n)])])
+        scratch_shapes=[
+            pltpu.VMEM(rows.shape, bf16),
+            pltpu.VMEM(floor_rate.shape, f32),
+            pltpu.VMEM(gains.shape, f32),
+            pltpu.SemaphoreType.DMA((n_in,)),
+        ],
+    )(at, *arrays)
 
 
 def reordered(blocks, odd, upper):
@@ -153,19 +164,20 @@
     halves = width // block
     kept = query_weight.shape[0]
 
-    spread, first, second, gain_pre, gain_post, head_gain, lower_bound, gain_mix = staged(
+    spread, first, second, gain_pre, gain_post, head_gain, gain_block, *floors = staged(
         unit,
         nz,
+        z_at.astype(jnp.int32)[None],
         [residual_in, gate_pre.T, up_pre.T],
         [down_pre, gate_post.T, up_post.T, down_post],
         [query_weight, forget_weight, value_weight, outgate_weight],
-        [v.reshape(-1, HEAD_DIM) for v in (gain_pre, gain_post, head_gain, lower_bound, gain_mix)],
+        [v.reshape(-1, HEAD_DIM) for v in (gain_pre, gain_post, head_gain)],
+        lower_bound.reshape(-1, HEAD_DIM),
+        gain_mix.reshape(-1, block),
     )
     gain_pre, gain_post = gain_pre.reshape(width), gain_post.reshape(width)
-    gain_block = lax.dynamic_slice_in_dim(gain_mix, z_at * block // HEAD_DIM, block // HEAD_DIM)
     gain_block = reordered(gain_block.reshape(ny, kept), y_at % 2 == 1, y_at // 2 == 1).reshape(block)
     first = from_others(first, "y")
-    second = doubled(second, "y", 2)
     middle = [*range(nz // 2, nz), *range(nz // 2)]
     all_rows = exchanged(spread, "z", [middle])
     all_rows = jnp.concatenate([all_rows[nz // 2 :], all_rows[: nz // 2]])
@@ -176,15 +188,13 @@
     elsewhere = (jnp.arange(nz, dtype=jnp.uint32) // halves != t_at)[:, None]
     note_at = t_at * halves
     odd, upper = y_at % 2 == 1, y_at // 2 == 1
-    floor_rate = lower_bound.reshape(-1, HEAD_DIM)
-    floors = (jnp.log(floor_rate), jnp.log1p(-floor_rate), 1.0 - floor_rate)
     all_rows, second, first, down_tiles, *known = lax.optimization_barrier(
         (all_rows, second, first, down_tiles, gain_block, gain_pre, gain_post, head_gain)
         + (*floors, mine, elsewhere, note_at, odd, upper, z_at)
     )
     gain_block, gain_pre, gain_post, head_gain, log_floor, log_rest, rest_rate = known[:7]
     mine, elsewhere, note_at, odd, upper, z_at = known[7:]
-    others = lax.ppermute(second, "y", [(i, i ^ 1) for i in range(ny)])
+    others = lax.ppermute(second, "y", [(i, i ^ 2) for i in range(ny)])
     gate_pre_t = first[:, :unit].reshape(ny * unit, width)
     up_pre_t = first[:, unit : 2 * unit].reshape(ny * unit, width)
 
@@ -196,21 +206,30 @@
         pieces = extra[:, : halves * piece].reshape(nz, piece, rows)
         return (
             lax.dynamic_index_in_dim(pieces, z_at, axis=0, keepdims=False),
+            jnp.concatenate([second, others]),
             *[extra[:, k * halves * piece :][:, : halves * piece].reshape(width, unit) for k in range(1, ny + 1)],
         )
 
-    hidden, (residual, *down_pre_t, second, gain_block) = hidden_units(
+    hidden, (residual, second, *down_pre_t, gain_block) = hidden_units(
         all_rows,
         gain_pre,
         gate_pre_t,
         up_pre_t,
         (turned.reshape(own_rows), down_tiles),
         finish,
-        (second, gain_block),
+        (gain_block,),
     )
     part = sum(
         dot(down_pre_t[k], hidden[k * unit : (k + 1) * unit], 1, 0) for k in range(ny)
     ).astype(bf16)
+    part, residual, second, gain_block = lax.optimization_barrier(
+        (part, residual, second, gain_block)
+    )
+    others = lax.ppermute(second, "y", [(i, i ^ 1) for i in range(ny)])
+    branch = exchanged(part.reshape(nz, piece, rows), "z")
+    branch = branch.astype(f32).sum(axis=0)
+    stream_piece = (residual.astype(f32) + 0.5 * branch).astype(bf16)
+
     second = jnp.concatenate([second, others]).reshape(ny, -1, width)
     gate_post_t, up_post_t, down_post_all = (
         second[:, k * unit : (k + 1) * unit].reshape(ny * unit, width) for k in range(3)
@@ -222,15 +241,9 @@
         ],
         axis=1,
     )
-    part, residual, gate_post_t, up_post_t, down_post_all, mixers, gain_block = (
-        lax.optimization_barrier(
-            (part, residual, gate_post_t, up_post_t, down_post_all, mixers, gain_block)
-        )
-    )
-    branch = exchanged(part.reshape(nz, piece, rows), "z")
-    branch = branch.astype(f32).sum(axis=0)
-    stream_piece = (residual.astype(f32) + 0.5 * branch).astype(bf16)
-
+    stream_piece, gate_post_t, up_post_t, down_post_all, mixers = lax.optimization_barrier(
+        (stream_piece, gate_post_t, up_post_t, down_post_all, mixers)
+    )
     stream_t = gathered(stream_piece, TP).reshape(block, rows)
     widened = stream_t.astype(f32)
     squares = jnp.sum(widened * widened, axis=0)

time: 189 us -> 194 us (1.026)
  blocking collectives: 123 us -> 105 us
  starting transfers between devices: 37.9 us -> 51.4 us
  waiting for transfers between devices: 13.4 us -> 18.9 us
  local copies, waits for them, and re-layouts: 4.09 us -> 7.42 us
    all_to_all x9 -> x8, blocking collectives: 123 us -> 105 us  [exchanged(): lax.all_to_all(tiles, axis, split_axis=0, concat_axis=0, axis_index_group...]
    all_to_all x2 -> x3, starting transfers between devices: 22.1 us -> 35.6 us  [exchanged(): lax.all_to_all(tiles, axis, split_axis=0, concat_axis=0, axis_index_group...]
    all_to_all x2 -> x3, waiting for transfers between devices: 2.7 us -> 10.2 us  [exchanged(): lax.all_to_all(tiles, axis, split_axis=0, concat_axis=0, axis_index_group...]
    ppermute x1, waiting for transfers between devices: 7.28 us -> 0.54 us  [shards(): others = lax.ppermute(second, 'y', [(i, i ^ 1) for i in range(ny)])]
    ppermute x1, waiting for transfers between devices: 3.36 us -> 8.22 us  [shards(): others = lax.ppermute(second, 'y', [(i, i ^ 2) for i in range(ny)])]
    unnamed x23 -> x29, local copies, waits for them, and re-layouts: 0.48 us -> 3.02 us
  transfers between devices with their start and end apart: 7 -> 8, of which waited for: 3 -> 4; matrix products, arithmetic and copies ran while one was open for 2% -> 1% of each run, Pallas kernels for 0% -> 0%
where the time goes in v6:
time: 194 us; the launch traced here: 193 us
  blocking collectives  105 us (54%)
  starting transfers between devices  51.4 us (26%)
  waiting for transfers between devices  18.9 us (10%)
  local copies, waits for them, and re-layouts  7.42 us (4%)
  other arithmetic  3.58 us (2%)
  matrix products  3.11 us (2%)
    all_to_all x8, blocking collectives, exchanged(): lax.all_to_all(tiles, axis, split_axis=0, concat_axis=0, axis_index_group...  105 us
    all_to_all x3, starting transfers between devices, exchanged(): lax.all_to_all(tiles, axis, split_axis=0, concat_axis=0, axis_index_group...  35.6 us
    ppermute x3, starting transfers between devices, from_others(): lax.ppermute(array, axis, [(i, (i - k) % n) for i in range(n)])  11.5 us
    all_to_all x3, waiting for transfers between devices, exchanged(): lax.all_to_all(tiles, axis, split_axis=0, concat_axis=0, axis_index_group...  10.2 us
    ppermute x1, waiting for transfers between devices, shards(): others = lax.ppermute(second, 'y', [(i, i ^ 2) for i in range(ny)])  8.22 us
  transfers between devices with their start and end apart: 8, of which 4 were waited for; matrix products, arithmetic and copies ran while one was open for 1% of the time, Pallas kernels for 0%

profile of v6, /device:TPU:1, one launch (start us, length us, event | category | flops | bytes accessed | tf_op | source)
XLA Modules:
  0.0 193.1 jit_solution(15046224920429325002)
XLA Ops:
  0.7 1.9 shard_map.185
  2.6 4.0 %collective-permute-start.2 = (bf16[288,256]{1,0:T(8,128)(2,1)}, bf16[288,256]{1,0:T(8,128)(2,1)S(1)}, u32[]{:S(2)}, u32[]{:S(2)}) collective-permute-start(bf16[288,256]{1,0:T(8,128)(2,1)} %get-tuple-element.50), channel_id=1, source_target_pairs={{0,8},{8,16},{16,24},{24,0},{1,9},{9,17},{17,25},{25,1},{2,10},{10... | collective-permute-start | bytes 442376 | tf_op jit(solution)/shard_map/ppermute | solution.py:34
  6.6 4.5 %collective-permute-start.1 = (bf16[288,256]{1,0:T(8,128)(2,1)}, bf16[288,256]{1,0:T(8,128)(2,1)S(1)}, u32[]{:S(2)}, u32[]{:S(2)}) collective-permute-start(bf16[288,256]{1,0:T(8,128)(2,1)} %get-tuple-element.50), channel_id=1, source_target_pairs={{0,16},{8,24},{16,0},{24,8},{1,17},{9,25},{17,1},{25,9},{2,18},{10... | collective-permute-start | bytes 442376 | tf_op jit(solution)/shard_map/ppermute | solution.py:34
  11.2 3.0 %collective-permute-start = (bf16[288,256]{1,0:T(8,128)(2,1)}, bf16[288,256]{1,0:T(8,128)(2,1)S(1)}, u32[]{:S(2)}, u32[]{:S(2)}) collective-permute-start(bf16[288,256]{1,0:T(8,128)(2,1)} %get-tuple-element.50), channel_id=1, source_target_pairs={{0,24},{8,0},{16,8},{24,16},{1,25},{9,1},{17,9},{25,17},{2,26},{10... | collective-permute-start | bytes 442376 | tf_op jit(solution)/shard_map/ppermute | solution.py:34
  14.1 18.3 %all-to-all-start = ((bf16[16,6,256]{2,1,0:T(8,128)(2,1)}), bf16[16,6,256]{2,1,0:T(8,128)(2,1)S(1)}, u32[]{:S(2)}, u32[]{:S(2)}) async-start(bf16[16,6,256]{2,1,0:T(8,128)(2,1)} %get-tuple-element.48), calls=%async_computation | async-start | bytes 131072 | tf_op jit(solution)/shard_map/all_to_all | solution.py:18
  32.5 0.9 fusion.41
  33.5 1.0 pad_maximum_fusion.1
  34.7 0.9 all-to-all-done
  39.3 0.7 constant_dynamic-update-slice_fusion
  40.1 6.9 %all-to-all-start.1 = ((bf16[8,264,96]{2,1,0:T(8,128)(2,1)}), bf16[8,264,96]{2,1,0:T(8,128)(2,1)S(1)}, u32[]{:S(2)}, u32[]{:S(2)}) async-start(bf16[8,264,96]{2,1,0:T(8,128)(2,1)} %constant_dynamic-update-slice_fusion), calls=%async_computation.1 | async-start | bytes 1081344 | tf_op jit(solution)/shard_map/all_to_all | solution.py:18
  47.0 1.9 %collective-permute-start.3 = (bf16[416,256]{1,0:T(8,128)(2,1)S(1)}, bf16[416,256]{1,0:T(8,128)(2,1)S(1)}, u32[]{:S(2)}, u32[]{:S(2)}) collective-permute-start(bf16[416,256]{1,0:T(8,128)(2,1)S(1)} %copy-done.3), channel_id=1, source_target_pairs={{0,16},{8,24},{16,0},{24,8},{1,17},{9,25},{17,1},{25,9},{2,18},{10... | collective-permute-start | bytes 638984 | tf_op jit(solution)/shard_map/ppermute | solution.py:197
  49.0 8.2 %collective-permute-done.3 = bf16[416,256]{1,0:T(8,128)(2,1)S(1)} collective-permute-done((bf16[416,256]{1,0:T(8,128)(2,1)S(1)}, bf16[416,256]{1,0:T(8,128)(2,1)S(1)}, u32[]{:S(2)}, u32[]{:S(2)}) %collective-permute-start.3) | collective-permute-done | bytes 213024 | tf_op jit(solution)/shard_map/ppermute | solution.py:197
  57.4 10.1 %all_to_all.55 = bf16[8,48,96]{2,1,0:T(8,128)(2,1)S(1)} all-to-all(bf16[8,48,96]{2,1,0:T(8,128)(2,1)S(1)} %broadcast_in_dim.56), channel_id=1, replica_groups=mesh['z'=16,'y'=4,'x'=4,'c'=2] {'x','c'}, dimensions={0} | all-to-all | bytes 147456 | tf_op jit(solution)/shard_map/all_to_all | solution.py:18
  69.1 10.3 %all-to-all-start.3 = ((bf16[16,16,96]{2,1,0:T(8,128)(2,1)}), bf16[16,16,96]{2,1,0:T(8,128)(2,1)S(1)}, u32[]{:S(2)}, u32[]{:S(2)}) async-start(bf16[16,16,96]{2,1,0:T(8,128)(2,1)} %bitcast.39), calls=%async_computation.3 | async-start | bytes 131072 | tf_op jit(solution)/shard_map/all_to_all | solution.py:18
  79.4 2.3 %collective-permute-start.4 = (bf16[832,256]{1,0:T(8,128)(2,1)S(1)}, bf16[832,256]{1,0:T(8,128)(2,1)S(1)}, u32[]{:S(2)}, u32[]{:S(2)}) collective-permute-start(bf16[832,256]{1,0:T(8,128)(2,1)S(1)} %pad_maximum_fusion.2), channel_id=1, source_target_pairs={{0,8},{8,0},{16,24},{24,16},{1,9},{9,1},{17,25},{25,17},{2,10},{10... | collective-permute-start | bytes 1277960 | tf_op jit(solution)/shard_map/ppermute | solution.py:228
  81.7 9.3 %all-to-all-done.3 = bf16[16,16,96]{2,1,0:T(8,128)(2,1)S(1)} async-done(((bf16[16,16,96]{2,1,0:T(8,128)(2,1)}), bf16[16,16,96]{2,1,0:T(8,128)(2,1)S(1)}, u32[]{:S(2)}, u32[]{:S(2)}) %all-to-all-start.3) | async-done | bytes 49184 | tf_op jit(solution)/shard_map/all_to_all | solution.py:18
  91.8 9.0 %all_to_all.56 = bf16[8,16,96]{2,1,0:T(8,128)(2,1)S(1)} all-to-all(bf16[8,16,96]{2,1,0:T(8,128)(2,1)S(1)} %broadcast_in_dim.57), channel_id=1, replica_groups=mesh['z'=16,'y'=4,'x'=4,'c'=2] {'x','c'}, dimensions={0} | all-to-all | bytes 49152 | tf_op jit(solution)/shard_map/all_to_all | solution.py:18
  101.9 24.0 %all_to_all.57 = bf16[16,54,128]{2,1,0:T(8,128)(2,1)S(1)} all-to-all(bf16[16,54,128]{2,1,0:T(8,128)(2,1)S(1)} %copy.131), channel_id=1, replica_groups=mesh['z'=16,'y'=4,'x'=4,'c'=2] {'z'}, dimensions={0} | all-to-all | bytes 442368 | tf_op jit(solution)/shard_map/all_to_all | solution.py:18
  127.1 0.8 fusion.21
  128.3 12.6 %all_to_all.58 = bf16[8,6,256]{2,1,0:T(8,128)(2,1)S(1)} all-to-all(bf16[8,6,256]{2,1,0:T(8,128)(2,1)S(1)} %bitcast.211), channel_id=1, replica_groups=mesh['z'=16,'y'=4,'x'=4,'c'=2] {'x','c'}, dimensions={0} | all-to-all | bytes 49152 | tf_op jit(solution)/shard_map/all_to_all | solution.py:18
  140.9 16.6 %all_to_all.59 = bf16[16,6,256]{2,1,0:T(8,128)(2,1)S(1)} all-to-all(bf16[16,6,256]{2,1,0:T(8,128)(2,1)S(1)} %broadcast_in_dim.62), channel_id=1, replica_groups=mesh['z'=16,'y'=4,'x'=4,'c'=2] {'z'}, dimensions={0} | all-to-all | bytes 98304 | tf_op jit(solution)/shard_map/all_to_all | solution.py:18
  158.7 10.4 %all_to_all.60 = bf16[8,104,96]{1,2,0:T(8,128)(2,1)S(1)} all-to-all(bf16[8,104,96]{1,2,0:T(8,128)(2,1)S(1)} %copy.139), channel_id=1, replica_groups=mesh['z'=16,'y'=4,'x'=4,'c'=2] {'x','c'}, dimensions={0} | all-to-all | bytes 319488 | tf_op jit(solution)/shard_map/all_to_all | solution.py:18
  169.6 8.3 %all_to_all.61 = bf16[8,48,96]{2,1,0:T(8,128)(2,1)S(1)} all-to-all(bf16[8,48,96]{2,1,0:T(8,128)(2,1)S(1)} %broadcast_in_dim.64), channel_id=1, replica_groups=mesh['z'=16,'y'=4,'x'=4,'c'=2] {'x','c'}, dimensions={0} | all-to-all | bytes 147456 | tf_op jit(solution)/shard_map/all_to_all | solution.py:18
  178.2 14.3 %all_to_all.62 = bf16[16,6,256]{2,1,0:T(8,128)(2,1)S(1)} all-to-all(bf16[16,6,256]{2,1,0:T(8,128)(2,1)S(1)} %reshape.268), channel_id=1, replica_groups=mesh['z'=16,'y'=4,'x'=4,'c'=2] {'z'}, dimensions={0} | all-to-all | bytes 98304 | tf_op jit(solution)/shard_map/all_to_all | solution.py:18
  (131 shorter events, 11.3 us)
Async XLA Ops:
  0.6 127.4 %copy-start = (bf16[256,2048]{1,0:T(8,128)(2,1)S(1)}, bf16[256,2048]{1,0:T(8,128)(2,1)}, u32[]{:S(2)}) copy-start(bf16[256,2048]{1,0:T(8,128)(2,1)} %param.30) | copy-start | bytes 3145732
  2.6 30.9 %collective-permute-start.2 = (bf16[288,256]{1,0:T(8,128)(2,1)}, bf16[288,256]{1,0:T(8,128)(2,1)S(1)}, u32[]{:S(2)}, u32[]{:S(2)}) collective-permute-start(bf16[288,256]{1,0:T(8,128)(2,1)} %get-tuple-element.50), channel_id=1, source_target_pairs={{0,8},{8,16},{16,24},{24,0},{1,9},{9,17},{17,25},{25,1},{2,10},{10... | collective-permute-start | bytes 442376 | tf_op jit(solution)/shard_map/ppermute | solution.py:34
  6.6 26.8 %collective-permute-start.1 = (bf16[288,256]{1,0:T(8,128)(2,1)}, bf16[288,256]{1,0:T(8,128)(2,1)S(1)}, u32[]{:S(2)}, u32[]{:S(2)}) collective-permute-start(bf16[288,256]{1,0:T(8,128)(2,1)} %get-tuple-element.50), channel_id=1, source_target_pairs={{0,16},{8,24},{16,0},{24,8},{1,17},{9,25},{17,1},{25,9},{2,18},{10... | collective-permute-start | bytes 442376 | tf_op jit(solution)/shard_map/ppermute | solution.py:34
  11.2 22.3 %collective-permute-start = (bf16[288,256]{1,0:T(8,128)(2,1)}, bf16[288,256]{1,0:T(8,128)(2,1)S(1)}, u32[]{:S(2)}, u32[]{:S(2)}) collective-permute-start(bf16[288,256]{1,0:T(8,128)(2,1)} %get-tuple-element.50), channel_id=1, source_target_pairs={{0,24},{8,0},{16,8},{24,16},{1,25},{9,1},{17,9},{25,17},{2,26},{10... | collective-permute-start | bytes 442376 | tf_op jit(solution)/shard_map/ppermute | solution.py:34
  14.1 21.4 %all-to-all-start = ((bf16[16,6,256]{2,1,0:T(8,128)(2,1)}), bf16[16,6,256]{2,1,0:T(8,128)(2,1)S(1)}, u32[]{:S(2)}, u32[]{:S(2)}) async-start(bf16[16,6,256]{2,1,0:T(8,128)(2,1)} %get-tuple-element.48), calls=%async_computation | async-start | bytes 131072 | tf_op jit(solution)/shard_map/all_to_all | solution.py:18
  34.5 1.2 copy-start.5
  37.4 9.6 %copy-start.3 = (bf16[416,256]{1,0:T(8,128)(2,1)S(1)}, bf16[416,256]{1,0:T(8,128)(2,1)}, u32[]{:S(2)}) copy-start(bf16[416,256]{1,0:T(8,128)(2,1)} %get-tuple-element.67) | copy-start | bytes 638980
  40.1 17.2 %all-to-all-start.1 = ((bf16[8,264,96]{2,1,0:T(8,128)(2,1)}), bf16[8,264,96]{2,1,0:T(8,128)(2,1)S(1)}, u32[]{:S(2)}, u32[]{:S(2)}) async-start(bf16[8,264,96]{2,1,0:T(8,128)(2,1)} %constant_dynamic-update-slice_fusion), calls=%async_computation.1 | async-start | bytes 1081344 | tf_op jit(solution)/shard_map/all_to_all | solution.py:18
  47.0 10.2 %collective-permute-start.3 = (bf16[416,256]{1,0:T(8,128)(2,1)S(1)}, bf16[416,256]{1,0:T(8,128)(2,1)S(1)}, u32[]{:S(2)}, u32[]{:S(2)}) collective-permute-start(bf16[416,256]{1,0:T(8,128)(2,1)S(1)} %copy-done.3), channel_id=1, source_target_pairs={{0,16},{8,24},{16,0},{24,8},{1,17},{9,25},{17,1},{25,9},{2,18},{10... | collective-permute-start | bytes 638984 | tf_op jit(solution)/shard_map/ppermute | solution.py:197
  69.1 21.9 %all-to-all-start.3 = ((bf16[16,16,96]{2,1,0:T(8,128)(2,1)}), bf16[16,16,96]{2,1,0:T(8,128)(2,1)S(1)}, u32[]{:S(2)}, u32[]{:S(2)}) async-start(bf16[16,16,96]{2,1,0:T(8,128)(2,1)} %bitcast.39), calls=%async_computation.3 | async-start | bytes 131072 | tf_op jit(solution)/shard_map/all_to_all | solution.py:18
  79.4 12.2 %collective-permute-start.4 = (bf16[832,256]{1,0:T(8,128)(2,1)S(1)}, bf16[832,256]{1,0:T(8,128)(2,1)S(1)}, u32[]{:S(2)}, u32[]{:S(2)}) collective-permute-start(bf16[832,256]{1,0:T(8,128)(2,1)S(1)} %pad_maximum_fusion.2), channel_id=1, source_target_pairs={{0,8},{8,0},{16,24},{24,16},{1,9},{9,1},{17,25},{25,17},{2,10},{10... | collective-permute-start | bytes 1277960 | tf_op jit(solution)/shard_map/ppermute | solution.py:228
  101.7 24.8 %copy-start.8 = (f32[2,128]{1,0:T(2,128)S(1)}, f32[2,128]{1,0:T(2,128)}, u32[]{:S(2)}) copy-start(f32[2,128]{1,0:T(2,128)} %get-tuple-element.88) | copy-start | bytes 3076
  101.7 24.9 %copy-start.6 = (f32[2,128]{1,0:T(2,128)S(1)}, f32[2,128]{1,0:T(2,128)}, u32[]{:S(2)}) copy-start(f32[2,128]{1,0:T(2,128)} %get-tuple-element.86) | copy-start | bytes 3076
  101.7 24.9 %copy-start.7 = (f32[2,128]{1,0:T(2,128)S(1)}, f32[2,128]{1,0:T(2,128)}, u32[]{:S(2)}) copy-start(f32[2,128]{1,0:T(2,128)} %get-tuple-element.87) | copy-start | bytes 3076
  101.7 24.9 %copy-start.2 = (f32[6,2,128,128]{3,2,1,0:T(8,128)S(1)}, f32[6,2,128,128]{3,2,1,0:T(8,128)}, u32[]{:S(2)}) copy-start(f32[6,2,128,128]{3,2,1,0:T(8,128)} %param.35) | copy-start | bytes 2359300
  126.6 1.4 copy-start.9
  127.1 13.8 %copy-start.1 = (f32[6,2,128,128]{3,2,1,0:T(8,128)}, f32[6,2,128,128]{3,2,1,0:T(8,128)S(1)}, u32[]{:S(2)}) copy-start(f32[6,2,128,128]{3,2,1,0:T(8,128)S(1)} %multiply_add_fusion) | copy-start | bytes 2359300
  127.1 30.7 %copy-start.4 = (f32[2,128]{1,0:T(2,128)S(1)}, f32[2,128]{1,0:T(2,128)}, u32[]{:S(2)}) copy-start(f32[2,128]{1,0:T(2,128)} %get-tuple-element.53) | copy-start | bytes 3076
